TPU v7x, 128 devices: a whole 4x4x4 slice. The times are simulated.
128 devices in a mesh: sp: 32 (over z, y, core), tp: 4 (over x).
Axes of the slice: x: 4, y: 4, z: 4, core: 2. Of those that a mesh axis runs over, the one named last changes fastest.
Arguments:
- query_nope: bfloat16 [6144, 4096], P('sp', 'tp'), may hold values from -6 to 6
- query_rope: bfloat16 [6144, 2048], P('sp', 'tp'), may hold values from -24 to 24
- latent: bfloat16 [6144, 512], P('sp'), may hold values from -6 to 6
- key_rope: bfloat16 [6144, 32], P('sp'), may hold values from -24 to 24
- latent_gain: float32 [512], replicated, may hold values from 0.1 to 1.9
- key_up: bfloat16 [512, 4096], P(None, 'tp'), may hold values from -0.25 to 0.25
- value_up: bfloat16 [512, 4096], P(None, 'tp'), may hold values from -0.25 to 0.25
- out_proj: bfloat16 [4096, 4096], P('tp'), may hold values from -0.09375 to 0.09375
- resid: bfloat16 [6144, 4096], P(('sp', 'tp')), may hold values from -6 to 6
- attn_gain: float32 [4096], replicated, may hold values from 0.1 to 1.9
- pre_gain: float32 [4096], replicated, may hold values from 0.1 to 1.9
- routes: int32 [6144, 2], P(('sp', 'tp')), may hold values from 0 to 31, all different within a row; in each aligned block of 48 rows (0 to 47, 48 to 95, ...) at most 6 rows name the same one
- route_weights: float32 [6144, 2], P(('sp', 'tp')), may hold values from 0.2 to 2
- expert_gate: bfloat16 [32, 4096, 1024], P('sp', None, 'tp'), may hold values from -0.09375 to 0.09375
- expert_up: bfloat16 [32, 4096, 1024], P('sp', None, 'tp'), may hold values from -0.09375 to 0.09375
- expert_down: bfloat16 [32, 1024, 4096], P('sp', 'tp'), may hold values from -0.1875 to 0.1875
- shared_gate: bfloat16 [4096, 1024], P(None, 'tp'), may hold values from -0.09375 to 0.09375
- shared_up: bfloat16 [4096, 1024], P(None, 'tp'), may hold values from -0.09375 to 0.09375
- shared_down: bfloat16 [1024, 4096], P('tp'), may hold values from -0.1875 to 0.1875
- moe_gain: float32 [4096], replicated, may hold values from 0.1 to 1.9
Outputs:
- output: bfloat16 [6144, 4096], P(('sp', 'tp'))
Inputs may be any that keep to these rules, and one draw needn't show every extreme that they name: `routes`: A row names 2 different experts. In each aligned block of 48 rows no expert is named by more than 6 rows, and in some block an expert is named by exactly 6 rows.
All inputs are finite; a program needn't handle non-finite values.
Results may differ from a plain program's by a relative error of at most 0.018.
Values may be sent and summed in bfloat16 or wider, within the bound.
No kernel may reach another device: no remote copies, remote signals or barrier semaphores. Data moves between devices by JAX's collectives and lax.ppermute only.
A program may use at most 128 MiB of HBM per device.

v0:
```python
import math

import jax
import jax.numpy as jnp
from jax import lax
from jax.sharding import PartitionSpec as P

MODEL_DIM = 4096
NOPE_DIM = 64
ROPE_DIM = 32
VALUE_DIM = 64
TOP_K = 2


epsilon = 1e-06
theta_base = 10000.0


def cut_along(array, dim, count):
    before, after = (array.shape[:dim], array.shape[dim + 1 :])
    return jnp.moveaxis(array.reshape(*before, count, -1, *after), dim, 0)


def sum_at_owner(array, axis, dim):
    count = lax.axis_size(axis)
    blocks = lax.all_to_all(cut_along(array, dim, count), axis, 0, 0, tiled=True)
    return jnp.sum(blocks.astype(jnp.float32), axis=0)


def rms_scale(values, gain_vector):
    return (
        values
        * lax.rsqrt(jnp.mean(values * values, axis=-1, keepdims=True) + epsilon)
        * gain_vector
    )


def rotate(values, positions):
    half_dim = values.shape[-1] // 2
    inverse = theta_base ** (-jnp.arange(half_dim, dtype=jnp.float32) / half_dim)
    angles = positions.astype(jnp.float32)[..., None] * inverse
    cosine = jnp.cos(angles)
    sine_part = jnp.sin(angles)
    first_half = values[..., :half_dim]
    second_half = values[..., half_dim:]
    return jnp.concatenate(
        [
            first_half * cosine - second_half * sine_part,
            second_half * cosine + first_half * sine_part,
        ],
        axis=-1,
    )


def expert_block(expert_in, gate_part, up_part, down_part):
    hidden = (
        jax.nn.silu(jnp.dot(expert_in, gate_part, preferred_element_type=jnp.float32))
        * jnp.dot(expert_in, up_part, preferred_element_type=jnp.float32)
    ).astype(jnp.bfloat16)
    return jnp.dot(hidden, down_part, preferred_element_type=jnp.float32).astype(jnp.bfloat16)


def dispatch_table(normed_rows, route_rows, experts, capacity):
    row_count = normed_rows.shape[0]
    flat_routes = route_rows.reshape(-1)
    onehot = (flat_routes[:, None] == jnp.arange(experts, dtype=jnp.int32)[None, :]).astype(
        jnp.int32
    )
    earlier = jnp.cumsum(onehot, axis=0) - onehot
    target = flat_routes * capacity + jnp.sum(earlier * onehot, axis=1)
    matches = (
        target.reshape(row_count, -1)[None, :, :]
        == jnp.arange(experts * capacity, dtype=jnp.int32)[:, None, None]
    )
    spread = jnp.any(matches, axis=2).astype(jnp.bfloat16)
    slot_table = jnp.dot(spread, normed_rows, preferred_element_type=jnp.float32).astype(
        jnp.bfloat16
    )
    return (slot_table.reshape(experts, capacity, normed_rows.shape[1]), target)


def on_device(
    query_nope,
    query_rope,
    latent,
    key_rope,
    latent_gain,
    key_up,
    value_up,
    out_proj,
    resid,
    attn_gain,
    pre_gain,
    routes,
    route_weights,
    expert_gate,
    expert_up,
    expert_down,
    shared_gate,
    shared_up,
    shared_down,
    moe_gain,
):
    local_rows = query_nope.shape[0]
    heads_here = query_nope.shape[1] // NOPE_DIM
    query_pos = lax.axis_index("sp") * local_rows + jnp.arange(local_rows, dtype=jnp.int32)
    last_query = lax.axis_index("sp") * local_rows + local_rows - 1
    query_rot = rotate(
        query_rope.astype(jnp.float32).reshape(local_rows, heads_here, ROPE_DIM), query_pos[:, None]
    ).astype(jnp.bfloat16)
    key_rot = rotate(key_rope.astype(jnp.float32), query_pos).astype(jnp.bfloat16)
    latent_normed = rms_scale(latent.astype(jnp.float32), latent_gain).astype(jnp.bfloat16)
    query_heads = query_nope.reshape(local_rows, heads_here, NOPE_DIM)
    score_scale = (NOPE_DIM + ROPE_DIM) ** (-0.5)

    def attend(state_now, latent_rows, rotary_rows, key_start):
        piece_rows = latent_rows.shape[0]
        keys_here = jnp.dot(latent_rows, key_up, preferred_element_type=jnp.float32).astype(
            jnp.bfloat16
        )
        keys_here = keys_here.reshape(piece_rows, heads_here, NOPE_DIM)
        values_here = jnp.dot(latent_rows, value_up, preferred_element_type=jnp.float32).astype(
            jnp.bfloat16
        )
        values_here = values_here.reshape(piece_rows, heads_here, VALUE_DIM)
        scores = (
            jnp.einsum("qhd,khd->hqk", query_heads, keys_here, preferred_element_type=jnp.float32)
            + jnp.einsum("qhr,kr->hqk", query_rot, rotary_rows, preferred_element_type=jnp.float32)
        ) * score_scale
        allowed = (key_start + jnp.arange(piece_rows, dtype=jnp.int32))[None, :] <= query_pos[
            :, None
        ]
        scores = jnp.where(allowed[None], scores, -1e30)
        running, total_sum, summed = state_now
        newest = jnp.maximum(running, jnp.max(scores, axis=-1))
        factor = jnp.exp(running - newest)
        exponent = jnp.exp(scores - newest[..., None])
        total_sum = total_sum * factor + jnp.sum(exponent, axis=-1)
        summed = summed * factor[..., None] + jnp.einsum(
            "hqk,khd->hqd",
            exponent.astype(jnp.bfloat16),
            values_here,
            preferred_element_type=jnp.float32,
        )
        return (newest, total_sum, summed)

    initial = (
        jnp.full((heads_here, local_rows), -1e30, jnp.float32),
        jnp.zeros((heads_here, local_rows), jnp.float32),
        jnp.zeros((heads_here, local_rows, VALUE_DIM), jnp.float32),
    )
    latent_piece = lax.all_gather(latent_normed, "sp", axis=0, tiled=True)
    rotary_piece = lax.all_gather(key_rot, "sp", axis=0, tiled=True)
    piece_rows = latent_piece.shape[0]
    step_rows = math.gcd(piece_rows, 512)

    def one_step(step_index, inner_state):
        offset = step_index * step_rows
        latent_rows = lax.dynamic_slice_in_dim(latent_piece, offset, step_rows, 0)
        rotary_rows = lax.dynamic_slice_in_dim(rotary_piece, offset, step_rows, 0)
        return lax.cond(
            offset <= last_query,
            lambda carried: attend(carried, latent_rows, rotary_rows, offset),
            lambda carried: carried,
            inner_state,
        )

    running, total_sum, summed = lax.fori_loop(0, piece_rows // step_rows, one_step, initial)
    attention = (
        (summed / total_sum[..., None])
        .transpose(1, 0, 2)
        .reshape(local_rows, heads_here * VALUE_DIM)
    )
    attention = attention.astype(jnp.bfloat16)
    projected = sum_at_owner(
        jnp.dot(attention, out_proj, preferred_element_type=jnp.float32).astype(jnp.bfloat16),
        "tp",
        0,
    )
    mixed = (resid.astype(jnp.float32) + rms_scale(projected, attn_gain)).astype(jnp.bfloat16)
    normed = rms_scale(mixed.astype(jnp.float32), pre_gain).astype(jnp.bfloat16)
    rows_here = resid.shape[0]
    tp_count = lax.axis_size("tp")
    experts = lax.axis_size("sp")
    capacity = max(2, 2 * rows_here * TOP_K // experts)
    own_table, target = dispatch_table(normed, routes, experts, capacity)
    arrived = lax.all_to_all(own_table, "sp", split_axis=0, concat_axis=0, tiled=True)
    column = lax.all_gather(arrived[None], "tp", axis=0, tiled=True)
    group_normed = lax.all_gather(normed, "tp", axis=0, tiled=True)
    expert_out = expert_block(
        column.reshape(-1, MODEL_DIM), expert_gate[0], expert_up[0], expert_down[0]
    )
    shared_part = expert_block(group_normed, shared_gate, shared_up, shared_down)
    routed_sum, shared_sum = (
        lax.psum_scatter(
            expert_out.reshape(column.shape).astype(jnp.float32).astype(jnp.bfloat16),
            "tp",
            scatter_dimension=0,
            tiled=True,
        ).astype(jnp.float32),
        lax.psum_scatter(
            shared_part.reshape(tp_count, rows_here, MODEL_DIM)
            .astype(jnp.float32)
            .astype(jnp.bfloat16),
            "tp",
            scatter_dimension=0,
            tiled=True,
        ).astype(jnp.float32),
    )
    expert_rows = lax.all_to_all(
        routed_sum.astype(jnp.bfloat16), "sp", split_axis=1, concat_axis=1, tiled=True
    ).reshape(-1, MODEL_DIM)
    shared_out = shared_sum.reshape(rows_here, MODEL_DIM)
    picked = expert_rows[target].astype(jnp.float32).reshape(rows_here, TOP_K, MODEL_DIM)
    routed = jnp.sum(picked * route_weights[..., None], axis=1)
    moe = shared_out + routed
    return (mixed.astype(jnp.float32) + rms_scale(moe, moe_gain)).astype(jnp.bfloat16)


def solution(mesh):
    in_specs = (
        P("sp", "tp"),
        P("sp", "tp"),
        P("sp", None),
        P("sp", None),
        P(),
        P(None, "tp"),
        P(None, "tp"),
        P("tp", None),
        P(("sp", "tp"), None),
        P(),
        P(),
        P(("sp", "tp"), None),
        P(("sp", "tp"), None),
        P("sp", None, "tp"),
        P("sp", None, "tp"),
        P("sp", "tp", None),
        P(None, "tp"),
        P(None, "tp"),
        P("tp", None),
        P(),
    )
    out_specs = P(("sp", "tp"), None)
    return jax.shard_map(
        on_device, mesh=mesh, in_specs=in_specs, out_specs=out_specs, check_vma=False
    )
```

profile of v0, /device:TPU:0, one launch (start us, length us, event | category | flops | bytes accessed | tf_op | source)
XLA Modules:
  0.0 656.6 jit_solution(17741494576442215457)
XLA Ops:
  12.1 26.5 %all-gather.1 = bf16[32,192,32]{1,2,0:T(8,128)(2,1)S(1)} all-gather(bf16[1,192,32]{1,2,0:T(8,128)(2,1)S(1)} %maximum_bitcast_fusion), channel_id=1, replica_groups=mesh['sp'=32,'tp'=4] {'sp'}, dimensions={0}, use_global_device_ids=true | all-gather | bytes 405504 | tf_op jit(solution)/shard_map/all_gather | solution.py:153
  42.0 19.7 %all-gather.6.cloned.1.call-done = bf16[6144,512]{1,0:T(8,128)(2,1)} async-done(((bf16[192,512]{1,0:T(8,128)(2,1)}), bf16[6144,512]{1,0:T(8,128)(2,1)}) %all-gather.6.cloned.1.call-update) | async-done | bytes 6291472 | tf_op jit(solution)/shard_map/all_gather | solution.py:152
  62.9 22.6 %while.18 = (s32[]{:T(128)}, f32[16,192]{1,0:T(8,128)S(1)}, f32[16,192]{1,0:T(8,128)S(1)}, f32[16,192,64]{1,2,0:T(8,128)}, s32[]{:T(128)}, /*index=5*/bf16[6144,...) while((s32[]{:T(128)}, f32[16,192]{1,0:T(8,128)S(1)}, ...), condition=%wide.region_6.7_spmd.clone, body=%wide.region_1.6_spmd.clone.sunk | while | flops 1591188224 | bytes 74948008 | solution.py:168
  62.9 22.1 %conditional.3 = ((f32[16,192]{1,0:T(8,128)S(1)}, f32[16,192]{1,0:T(8,128)S(1)}, f32[16,192,64]{1,2,0:T(8,128)})) conditional(s32[]{:T(128)} %convert_element_type.188, (f32[16,192]{1,0:T(8,128)S(1)}, f32[16,192]{1,0:T(8,128)S(1)}, f32[16,192,64]{1,2,0:T(8,128)}) %tuple.60, (s32[]{:T(128)}, s32[]{:T(128)}, bf16[6144,512]{1,0:T(8,128)(2,1)}, ...), branch_computations={%region_2.0_spmd, %region_3.5_spmd} | conditional | flops 1591188224 | bytes 74946960 | solution.py:161
  62.9 3.2 convolution_convert_fusion.1
  79.6 5.4 fusion.9
  86.8 6.4 convolution_convert_fusion.5
  93.2 4.5 all-to-all-start
  98.9 20.2 %all-to-all-done = bf16[4,48,4096]{2,1,0:T(8,128)(2,1)} async-done(((bf16[4,48,4096]{2,1,0:T(8,128)(2,1)}), bf16[4,48,4096]{2,1,0:T(8,128)(2,1)}, u32[]{:S(2)}, u32[]{:S(2)}) %all-to-all-start) | async-done | bytes 1572896 | tf_op jit(solution)/shard_map/all_to_all | solution.py:26
  123.4 3.5 reshape.247
  126.9 275.5 %all_to_all.15 = bf16[32,6,4096]{2,1,0:T(8,128)(2,1)S(1)} all-to-all(bf16[32,6,4096]{2,1,0:T(8,128)(2,1)} %reshape.247), channel_id=1, replica_groups=mesh['sp'=32,'tp'=4] {'sp'}, dimensions={0} | all-to-all | bytes 3145728 | tf_op jit(solution)/shard_map/all_to_all | solution.py:187
  405.2 60.8 %all-gather.10.cloned.1.call-done = bf16[128,6,4096]{2,0,1:T(8,128)(2,1)} async-done(((bf16[32,6,4096]{2,0,1:T(8,128)(2,1)}), bf16[128,6,4096]{2,0,1:T(8,128)(2,1)}) %all-gather.10.cloned.1.call-update) | async-done | bytes 6291472 | tf_op jit(solution)/shard_map/all_gather | solution.py:188
  466.1 9.6 %copy.67 = bf16[128,6,4096]{2,1,0:T(8,128)(2,1)} copy(bf16[128,6,4096]{2,0,1:T(8,128)(2,1)} %all-gather.10.cloned.1.call-done) | data formatting | bytes 12582912 | tf_op jit(solution)/shard_map/all_gather | solution.py:188
  475.6 10.3 %reshape.248 = bf16[768,4096]{1,0:T(8,128)(2,1)} reshape(bf16[128,6,4096]{2,1,0:T(8,128)(2,1)} %copy.67) | data formatting | bytes 12582912 | tf_op jit(solution)/shard_map/reshape | solution.py:191
  486.0 6.2 fusion.22
  492.2 12.8 %convolution_convert_fusion.2 = bf16[768,4096]{1,0:T(8,128)(2,1)} fusion(bf16[1,256,4096]{2,1,0:T(8,128)(2,1)S(1)} %copy-done, bf16[768,4096]{1,0:T(8,128)(2,1)} %reshape.248, bf16[1,4096,256]{2,1,0:T(8,128)(2,1)} %param.38, f32[768,256]{1,0:T(8,128)} %fusion.22), kind=kOutput, calls=%fused_computation.25 | convolution fusion | flops 3225550848 | bytes 17563648 | tf_op jit(solution)/shard_map/dot_general | solution.py:60
  505.0 10.1 %reshape.249 = bf16[4,32,6,4096]{3,2,1,0:T(8,128)(2,1)} reshape(bf16[768,4096]{1,0:T(8,128)(2,1)} %convolution_convert_fusion.2) | data formatting | bytes 12582912 | tf_op jit(solution)/shard_map/reshape | solution.py:196
  518.1 5.7 convolution_convert_fusion.4
  523.8 72.6 %reduce-scatter.5.cloned.1.call-done = bf16[1,32,6,4096]{3,2,1,0:T(8,128)(2,1)} async-done(((bf16[4,32,6,4096]{3,2,1,0:T(8,128)(2,1)}), bf16[1,32,6,4096]{3,2,1,0:T(8,128)(2,1)}) %reduce-scatter.5.cloned.1.call-update) | async-done | bytes 1572880 | tf_op jit(solution)/shard_map/reduce_scatter | solution.py:195
  596.5 7.5 %all-to-all-start.2 = ((bf16[1,32,6,4096]{3,2,0,1:T(8,128)(2,1)}), bf16[1,32,6,4096]{3,2,0,1:T(8,128)(2,1)}, u32[]{:S(2)}, u32[]{:S(2)}) async-start(bf16[1,32,6,4096]{3,2,0,1:T(8,128)(2,1)} %bitcast.77), calls=%async_computation.4 | async-start | bytes 4194304 | tf_op jit(solution)/shard_map/all_to_all | solution.py:210
  604.2 29.8 %all-to-all-done.2 = bf16[1,32,6,4096]{3,2,0,1:T(8,128)(2,1)} async-done(((bf16[1,32,6,4096]{3,2,0,1:T(8,128)(2,1)}), bf16[1,32,6,4096]{3,2,0,1:T(8,128)(2,1)}, u32[]{:S(2)}, u32[]{:S(2)}) %all-to-all-start.2) | async-done | bytes 1572896 | tf_op jit(solution)/shard_map/all_to_all | solution.py:210
  634.0 3.7 reshape.250
  637.7 3.4 gather_fusion
  643.2 3.6 multiply_reduce_fusion
  (113 shorter events, 41.7 us)
Async XLA Ops:
  6.5 485.7 %copy-start = (bf16[1,256,4096]{2,1,0:T(8,128)(2,1)S(1)}, bf16[1,256,4096]{2,1,0:T(8,128)(2,1)}, u32[]{:S(2)}) copy-start(bf16[1,256,4096]{2,1,0:T(8,128)(2,1)} %param.39) | copy-start | bytes 6291460
  6.5 33.6 %copy-start.3 = (bf16[192,1024]{1,0:T(8,128)(2,1)S(1)}, bf16[192,1024]{1,0:T(8,128)(2,1)}, u32[]{:S(2)}) copy-start(bf16[192,1024]{1,0:T(8,128)(2,1)} %param.24) | copy-start | bytes 1179652
  6.5 55.2 %all-gather.6.cloned.1.call-start = ((), (), s32[]{:S(2)}) async-start(), calls=%async_computation.5 | async-start | bytes 6488064 | tf_op jit(solution)/shard_map/all_gather | solution.py:152
  72.6 2.7 copy-start.1
  72.7 2.7 copy-start.10
  93.2 4.7 copy-start.8
  93.2 25.9 %all-to-all-start = ((bf16[4,48,4096]{2,1,0:T(8,128)(2,1)}), bf16[4,48,4096]{2,1,0:T(8,128)(2,1)}, u32[]{:S(2)}, u32[]{:S(2)}) async-start(bf16[4,48,4096]{2,1,0:T(8,128)(2,1)} %bitcast.75), calls=%async_computation | async-start | bytes 3145728 | tf_op jit(solution)/shard_map/all_to_all | solution.py:26
  97.7 23.4 %copy-start.4 = (bf16[48,4096]{1,0:T(8,128)(2,1)S(1)}, bf16[48,4096]{1,0:T(8,128)(2,1)}, u32[]{:S(2)}) copy-start(bf16[48,4096]{1,0:T(8,128)(2,1)} %param.32) | copy-start | bytes 1179652
  97.7 23.4 %copy-start.5 = (f32[4096]{0:T(1024)S(1)}, f32[4096]{0:T(1024)}, u32[]{:S(2)}) copy-start(f32[4096]{0:T(1024)} %param.33) | copy-start | bytes 49156
  97.7 368.4 %all-gather.10.cloned.1.call-start = ((), (), s32[]{:S(2)}) async-start(), calls=%async_computation.9 | async-start | bytes 7864320 | tf_op jit(solution)/shard_map/all_gather | solution.py:188
  98.9 22.5 %copy-start.7 = (f32[4096]{0:T(1024)S(1)}, f32[4096]{0:T(1024)}, u32[]{:S(2)}) copy-start(f32[4096]{0:T(1024)} %param.34) | copy-start | bytes 49156
  121.6 5.3 copy-start.2
  404.5 111.0 %all-gather.8.cloned.1.call-start = ((), (), s32[]{:S(2)}) async-start(), calls=%async_computation.6 | async-start | bytes 1966080 | tf_op jit(solution)/shard_map/all_gather | solution.py:189
  405.2 191.3 %reduce-scatter.5.cloned.1.call-start = ((), (), s32[]{:S(2)}) async-start(), calls=%async_computation.8 | async-start | bytes 10485760 | tf_op jit(solution)/shard_map/reduce_scatter | solution.py:195
  515.1 131.7 %reduce-scatter.3.cloned.1.call-start = ((), (), s32[]{:S(2)}) async-start(), calls=%async_computation.7 | async-start | bytes 1966080 | tf_op jit(solution)/shard_map/reduce_scatter | solution.py:201
  596.5 7.6 %copy-start.9 = (f32[48,2]{0,1:T(2,128)S(1)}, f32[48,2]{0,1:T(2,128)}, u32[]{:S(2)}) copy-start(f32[48,2]{0,1:T(2,128)} %param.36) | copy-start | bytes 1156
  596.5 37.6 %all-to-all-start.2 = ((bf16[1,32,6,4096]{3,2,0,1:T(8,128)(2,1)}), bf16[1,32,6,4096]{3,2,0,1:T(8,128)(2,1)}, u32[]{:S(2)}, u32[]{:S(2)}) async-start(bf16[1,32,6,4096]{3,2,0,1:T(8,128)(2,1)} %bitcast.77), calls=%async_computation.4 | async-start | bytes 4194304 | tf_op jit(solution)/shard_map/all_to_all | solution.py:210
  643.2 4.9 copy-start.6
Sparse Core Ops, SparseCore 0:
  9.6 52.0 all-gather.5
  404.6 61.4 all-gather.9
  467.8 27.0 all-gather.7
  515.3 81.1 reduce-scatter.4
  598.7 25.3 reduce-scatter.2
where the time goes:
time: 661 us; the launch traced here: 657 us
  blocking collectives  302 us (46%)
  waiting for transfers between devices  204 us (31%)
  local copies, waits for them, and re-layouts  54.2 us (8%)
  matrix products  51.7 us (8%)
  other arithmetic  18.1 us (3%)
  between operations  13.4 us (2%)
  starting transfers between devices  12.5 us (2%)
    all_to_all x1, blocking collectives, on_device(): lax.all_to_all(own_table, 'sp', split_axis=0, concat_axis=0, tiled=True)  275 us
    reduce_scatter x1, waiting for transfers between devices, on_device(): lax.psum_scatter(expert_out.reshape(column.shape).astype(jnp.float32).ast...  72.6 us
    all_gather x1, waiting for transfers between devices, on_device(): column = lax.all_gather(arrived[None], 'tp', axis=0, tiled=True)  60.8 us
    all_to_all x1, waiting for transfers between devices, on_device(): lax.all_to_all(routed_sum.astype(jnp.bfloat16), 'sp', split_axis=1, conca...  29.8 us
    all_gather x1, blocking collectives, on_device(): rotary_piece = lax.all_gather(key_rot, 'sp', axis=0, tiled=True)  26.5 us
    all_to_all x1, waiting for transfers between devices, sum_at_owner(): lax.all_to_all(cut_along(array, dim, count), axis, 0, 0, tiled=True)  20.2 us
    all_gather x1, waiting for transfers between devices, on_device(): latent_piece = lax.all_gather(latent_normed, 'sp', axis=0, tiled=True)  19.7 us
    dot_general x2, matrix products, expert_block(): jnp.dot(hidden, down_part, preferred_element_type=jnp.float32)  18.5 us
  transfers between devices with their start and end apart: 7, of which 5 were waited for; matrix products, arithmetic and copies ran while one was open for 12% of the time, Pallas kernels for 0%

commit v1 on v0

v1 whole, which is shorter than its diff:
```python
import functools

import jax
import jax.numpy as jnp
from jax import lax
from jax.experimental import pallas as pl
from jax.experimental.pallas import tpu as pltpu
from jax.sharding import PartitionSpec as P


MODEL_DIM = 4096
NOPE_DIM = 64
ROPE_DIM = 32
VALUE_DIM = 64
TOP_K = 2


epsilon = 1e-06
theta_base = 10000.0


def cut_along(array, dim, count):
    before, after = (array.shape[:dim], array.shape[dim + 1 :])
    return jnp.moveaxis(array.reshape(*before, count, -1, *after), dim, 0)


def sum_at_owner(array, axis, dim):
    count = lax.axis_size(axis)
    blocks = lax.all_to_all(cut_along(array, dim, count), axis, 0, 0, tiled=True)
    return jnp.sum(blocks.astype(jnp.float32), axis=0)


def rms_scale(values, gain_vector):
    return (
        values
        * lax.rsqrt(jnp.mean(values * values, axis=-1, keepdims=True) + epsilon)
        * gain_vector
    )


def rotate(values, positions):
    half_dim = values.shape[-1] // 2
    inverse = theta_base ** (-jnp.arange(half_dim, dtype=jnp.float32) / half_dim)
    angles = positions.astype(jnp.float32)[..., None] * inverse
    cosine = jnp.cos(angles)
    sine_part = jnp.sin(angles)
    first_half = values[..., :half_dim]
    second_half = values[..., half_dim:]
    return jnp.concatenate(
        [
            first_half * cosine - second_half * sine_part,
            second_half * cosine + first_half * sine_part,
        ],
        axis=-1,
    )


def gate_kernel(x_ref, w_ref, out_ref):
    out_ref[0] = jnp.dot(x_ref[...], w_ref[0], preferred_element_type=jnp.float32).astype(
        out_ref.dtype
    )


def gate_call(x, weights):
    quarters, _, width = weights.shape
    rows, depth = x.shape
    return pl.pallas_call(
        gate_kernel,
        grid=(quarters,),
        out_shape=jax.ShapeDtypeStruct((quarters, rows, width), jnp.bfloat16),
        in_specs=[
            pl.BlockSpec((rows, depth), lambda q: (0, 0)),
            pl.BlockSpec((1, depth, width), lambda q: (q, 0, 0)),
        ],
        out_specs=pl.BlockSpec((1, rows, width), lambda q: (q, 0, 0)),
        compiler_params=pltpu.CompilerParams(vmem_limit_bytes=40 * 1024 * 1024),
        cost_estimate=pl.CostEstimate(
            flops=2 * rows * depth * width * quarters, bytes_accessed=9_000_000, transcendentals=0
        ),
    )(x, weights)


def down_kernel(hidden_ref, w_ref, routed_ref, shared_ref):
    quarters = hidden_ref.shape[0]
    half = w_ref.shape[1] // 2
    routed_rows = routed_ref.shape[0]
    routed = shared = 0.0
    for q in range(quarters):
        routed += jnp.dot(
            hidden_ref[q, :routed_rows], w_ref[q, :half], preferred_element_type=jnp.float32
        )
        shared += jnp.dot(
            hidden_ref[q, routed_rows:], w_ref[q, half:], preferred_element_type=jnp.float32
        )
    routed_ref[...] = routed.astype(routed_ref.dtype)
    shared_ref[...] = shared


def down_call(hidden, weights, routed_rows, cols):
    quarters, rows, half = hidden.shape
    tile = weights.shape[2]
    first = (weights.shape[1] - 2 * half * cols // tile) // (2 * half)
    return pl.pallas_call(
        down_kernel,
        grid=(cols // tile,),
        out_shape=(
            jax.ShapeDtypeStruct((routed_rows, cols), jnp.bfloat16),
            jax.ShapeDtypeStruct((rows - routed_rows, cols), jnp.float32),
        ),
        in_specs=[
            pl.BlockSpec((quarters, rows, half), lambda n: (0, 0, 0)),
            pl.BlockSpec((quarters, 2 * half, tile), lambda n: (0, first + n, 0)),
        ],
        out_specs=(
            pl.BlockSpec((routed_rows, tile), lambda n: (0, n)),
            pl.BlockSpec((rows - routed_rows, tile), lambda n: (0, n)),
        ),
        compiler_params=pltpu.CompilerParams(vmem_limit_bytes=40 * 1024 * 1024),
        cost_estimate=pl.CostEstimate(
            flops=2 * rows * half * quarters * cols, bytes_accessed=8_000_000, transcendentals=0
        ),
    )(hidden, weights)


def slot_tables(routes, weights, experts, capacity):
    blocks, rows, picks = routes.shape
    flat = routes.reshape(blocks, rows * picks)
    onehot = (flat[..., None] == jnp.arange(experts, dtype=jnp.int32)).astype(jnp.int32)
    earlier = jnp.cumsum(onehot, axis=1) - onehot
    target = flat * (blocks * capacity) + jnp.sum(earlier * onehot, axis=-1)
    target = target + jnp.arange(blocks, dtype=jnp.int32)[:, None] * capacity
    target = target.reshape(blocks * rows, picks)
    slots = jnp.arange(experts * blocks * capacity, dtype=jnp.int32)
    spread = jnp.any(target.T[:, None, :] == slots[None, :, None], axis=0).astype(jnp.bfloat16)
    shares = jnp.sum(
        jnp.where(
            target[:, :, None] == slots[None, None, :],
            weights.reshape(blocks * rows, picks)[..., None],
            0.0,
        ),
        axis=1,
    )
    high = lax.reduce_precision(shares, 8, 7)
    return spread, high.astype(jnp.bfloat16), (shares - high).astype(jnp.bfloat16)


def far_pairs(groups, pairs):
    counts = []
    for low in range(groups // 2):
        mine, theirs = low // 2 + 2.1, (groups - 1 - low) // 2 + 2.1
        best = min(
            range(pairs // 2 + 1),
            key=lambda n: max(pairs * mine + n * theirs, (pairs - n) * theirs),
        )
        counts.append(best)
    return counts


LOG2E = 1.4426950408889634
PACK_ROWS = 16


def attention_kernel(
    desc_ref, gath_ref, qt_ref, ku_ref, vu_ref, out_ref, rot_ref, w_ref, *, block, score_scale
):
    devices, grows, lat_dim = gath_ref.shape
    rows = grows - PACK_ROWS
    per = block // rows
    width = qt_ref.shape[2]
    half = width // 2
    factor = score_scale * LOG2E
    rot_ref[...] = jnp.zeros_like(rot_ref)

    def unpack(d, _):
        packed = gath_ref[d, rows:grows, :]
        for g in range(rows // PACK_ROWS):
            rot_ref[d, g * PACK_ROWS : (g + 1) * PACK_ROWS, 0:ROPE_DIM] = packed[
                :, g * ROPE_DIM : (g + 1) * ROPE_DIM
            ]
        return 0

    lax.fori_loop(0, devices, unpack, 0)
    n_own, i_own, n_far, i_far = desc_ref[0], desc_ref[1], desc_ref[2], desc_ref[3]
    pairs = ku_ref.shape[1] // 128
    extra = qt_ref.shape[0] - pairs

    def one_pair(u, _):
        far = u >= n_own
        pair = jnp.where(far, pairs - n_far + (u - n_own), u)
        slot = jnp.where(far, pair + extra, pair)
        index = jnp.where(far, i_far, i_own)
        col = pl.multiple_of(pair * 128, 128)
        w_ref[:, 0:128] = ku_ref[:, pl.ds(col, 128)]
        w_ref[:, 128:256] = vu_ref[:, pl.ds(col, 128)]

        def scores(b):
            lat = gath_ref[pl.ds(b * per, per), 0:rows, :].reshape(block, lat_dim)
            kv = jnp.dot(lat, w_ref[...], preferred_element_type=jnp.float32).astype(jnp.bfloat16)
            rot = rot_ref[pl.ds(b * per, per)].reshape(block, 128)
            keys = jnp.concatenate([kv[:, :128], rot], axis=1)
            s = jnp.dot(keys, qt_ref[slot], preferred_element_type=jnp.float32)
            return s, kv[:, 128:]

        def weigh(v, p):
            return lax.dot_general(
                v,
                p.astype(jnp.bfloat16),
                (((0,), (0,)), ((), ())),
                preferred_element_type=jnp.float32,
            )

        full = (index * rows) // block
        s, v = scores(full)
        key = lax.broadcasted_iota(jnp.int32, (block, width), 0) + full * block
        lane = lax.broadcasted_iota(jnp.int32, (block, width), 1)
        query = index * rows + jnp.where(lane >= half, lane - half, lane)
        s = jnp.where(key <= query, s, -1e30)
        top = jnp.max(s, axis=0, keepdims=True)
        p = jnp.exp2(s * factor - top * factor)
        state = (top, jnp.sum(p, axis=0, keepdims=True), weigh(v, p))

        def update(state, s, v):
            top, total, acc = state
            newest = jnp.maximum(top, jnp.max(s, axis=0, keepdims=True))
            alpha = jnp.exp2((top - newest) * factor)
            p = jnp.exp2(s * factor - newest * factor)
            total = total * alpha + jnp.sum(p, axis=0, keepdims=True)
            return newest, total, acc * alpha + weigh(v, p)

        def two(b, state):
            first, second = scores(b * 2), scores(b * 2 + 1)
            return update(update(state, *first), *second)

        state = lax.fori_loop(0, full // 2, two, state)
        state = lax.fori_loop(
            (full // 2) * 2, full, lambda b, state: update(state, *scores(b)), state
        )
        top, total, acc = state
        res = acc / total
        out_ref[slot, 0:64, :] = res[0:64, 0:half].astype(jnp.bfloat16)
        out_ref[slot, 64:128, :] = res[64:128, half:].astype(jnp.bfloat16)
        return 0

    lax.fori_loop(0, n_own + n_far, one_pair, 0)


def attention_call(desc, gathered, qt, key_up, value_up, score_scale):
    devices, grows, lat_dim = gathered.shape
    rows = grows - PACK_ROWS
    slots, _, width = qt.shape
    return pl.pallas_call(
        functools.partial(attention_kernel, block=rows * 2, score_scale=score_scale),
        out_shape=jax.ShapeDtypeStruct((slots, 128, width // 2), jnp.bfloat16),
        in_specs=[pl.BlockSpec(memory_space=pltpu.SMEM)]
        + [pl.BlockSpec(memory_space=pltpu.VMEM)] * 4,
        out_specs=pl.BlockSpec(memory_space=pltpu.VMEM),
        scratch_shapes=[
            pltpu.VMEM((devices, rows, 128), jnp.bfloat16),
            pltpu.VMEM((lat_dim, 256), jnp.bfloat16),
        ],
        compiler_params=pltpu.CompilerParams(vmem_limit_bytes=50 * 1024 * 1024),
        cost_estimate=pl.CostEstimate(
            flops=50_000_000_000, bytes_accessed=12_000_000, transcendentals=20_000_000
        ),
    )(desc, gathered, qt, key_up, value_up)


def query_tiles(query_nope, query_rot):
    rows = query_nope.shape[0]
    pairs = query_nope.shape[1] // (2 * NOPE_DIM)
    nope = query_nope.reshape(rows, pairs, 2, NOPE_DIM).transpose(1, 2, 3, 0)
    rot = query_rot.reshape(rows, pairs, 2, ROPE_DIM).transpose(1, 2, 3, 0)
    none = jnp.zeros_like(nope[:, 0])
    return jnp.concatenate(
        [
            jnp.concatenate([nope[:, 0], none], axis=2),
            jnp.concatenate([none, nope[:, 1]], axis=2),
            jnp.concatenate([rot[:, 0], rot[:, 1]], axis=2),
            jnp.zeros((pairs, 128 - ROPE_DIM, 2 * rows), query_nope.dtype),
        ],
        axis=1,
    )


def layer(
    query_nope,
    query_rope,
    latent,
    key_rope,
    latent_gain,
    key_up,
    value_up,
    out_proj,
    resid,
    attn_gain,
    pre_gain,
    routes,
    route_weights,
    expert_gate,
    expert_up,
    expert_down,
    shared_gate,
    shared_up,
    shared_down,
    moe_gain,
):
    local_rows = query_nope.shape[0]
    heads_here = query_nope.shape[1] // NOPE_DIM
    query_pos = lax.axis_index("sp") * local_rows + jnp.arange(local_rows, dtype=jnp.int32)
    query_rot = rotate(
        query_rope.astype(jnp.float32).reshape(local_rows, heads_here, ROPE_DIM), query_pos[:, None]
    ).astype(jnp.bfloat16)
    key_rot = rotate(key_rope.astype(jnp.float32), query_pos).astype(jnp.bfloat16)
    latent_normed = rms_scale(latent.astype(jnp.float32), latent_gain).astype(jnp.bfloat16)
    score_scale = (NOPE_DIM + ROPE_DIM) ** (-0.5)

    groups = lax.axis_size("sp")
    place = lax.axis_index("sp").astype(jnp.int32)
    tp_count = lax.axis_size("tp")
    pairs = heads_here // 2
    far = pairs // 2
    cols = MODEL_DIM // tp_count
    rows_here = resid.shape[0]
    capacity = max(2, 2 * rows_here * TOP_K // groups)
    group_rows = tp_count * rows_here

    sent_queries = jnp.concatenate(
        [
            query_nope[:, far * 2 * NOPE_DIM :],
            query_rot.reshape(local_rows, -1)[:, far * 2 * ROPE_DIM :],
        ],
        axis=1,
    )
    down_pairs = [(groups - 1 - low, low) for low in range(groups // 2)]
    far_queries = lax.ppermute(sent_queries, "sp", down_pairs)

    packed_rot = key_rot.reshape(local_rows // PACK_ROWS, PACK_ROWS, ROPE_DIM).transpose(1, 0, 2)
    packed_rot = packed_rot.reshape(PACK_ROWS, -1)
    packed_rot = jnp.pad(packed_rot, ((0, 0), (0, latent.shape[1] - packed_rot.shape[1])))
    gathered = lax.all_gather(
        jnp.concatenate([latent_normed, packed_rot], axis=0), "sp", axis=0, tiled=False
    )

    route_data = lax.all_gather(
        jnp.concatenate([routes.astype(jnp.float32), route_weights], axis=1), "tp", axis=0
    )
    gate_up = jnp.concatenate([expert_gate[0], expert_up[0]], axis=1)
    gate_width = gate_up.shape[1]
    gate_up = gate_up.reshape(tp_count, cols, gate_width)
    downs = jnp.concatenate([expert_down[0], shared_down], axis=0)
    downs = downs.reshape(downs.shape[0], tp_count, cols // gate_width, gate_width)
    downs = downs.transpose(1, 2, 0, 3).reshape(tp_count, -1, gate_width)
    gate_up, downs, route_data = lax.optimization_barrier((gate_up, downs, route_data))
    weights = lax.all_to_all(
        jnp.concatenate([gate_up, downs], axis=1), "tp", split_axis=0, concat_axis=0, tiled=True
    )
    spread, share_high, share_low = slot_tables(
        route_data[..., :TOP_K].astype(jnp.int32), route_data[..., TOP_K:], groups, capacity
    )

    is_low = place < groups // 2
    low_place = jnp.minimum(place, groups - 1 - place)
    moved = jnp.asarray(far_pairs(groups, pairs), jnp.int32)[low_place]
    n_own = jnp.where(is_low, pairs, pairs - moved)
    desc = jnp.stack([n_own, place, jnp.where(is_low, moved, 0), groups - 1 - place])
    tiles = jnp.concatenate(
        [
            query_tiles(query_nope, query_rot),
            query_tiles(
                far_queries[:, : far * 2 * NOPE_DIM], far_queries[:, far * 2 * NOPE_DIM :]
            ),
        ],
        axis=0,
    )
    desc, spread, share_high, share_low = lax.optimization_barrier(
        (desc, spread, share_high, share_low)
    )
    attended = attention_call(desc, gathered, tiles, key_up, value_up, score_scale)
    returned = lax.ppermute(attended[pairs:], "sp", [(low, high) for high, low in down_pairs])
    pair_ids = jnp.arange(pairs - far, pairs, dtype=jnp.int32)[:, None, None]
    attended = jnp.concatenate(
        [
            attended[: pairs - far],
            jnp.where(pair_ids < n_own, attended[pairs - far : pairs], returned),
        ],
        axis=0,
    ).reshape(heads_here * VALUE_DIM, local_rows)
    partial = lax.dot_general(
        attended, out_proj, (((0,), (0,)), ((), ())), preferred_element_type=jnp.float32
    ).astype(jnp.bfloat16)
    projected = sum_at_owner(partial, "tp", 0)
    mixed = (resid.astype(jnp.float32) + rms_scale(projected, attn_gain)).astype(jnp.bfloat16)
    normed = rms_scale(mixed.astype(jnp.float32), pre_gain).astype(jnp.bfloat16)

    columns = lax.all_to_all(
        normed.reshape(rows_here, tp_count, cols).transpose(1, 0, 2),
        "tp",
        split_axis=0,
        concat_axis=0,
        tiled=True,
    ).reshape(group_rows, cols)
    group_normed = lax.all_gather(normed, "tp", axis=0, tiled=True)
    table = jnp.dot(spread, columns, preferred_element_type=jnp.float32).astype(jnp.bfloat16)
    slots = table.shape[0]
    arrived = lax.all_to_all(
        table.reshape(groups, -1, cols), "sp", split_axis=0, concat_axis=0, tiled=True
    ).reshape(slots, cols)
    partial = gate_call(arrived, weights)
    gated = lax.psum_scatter(partial, "tp", scatter_dimension=0, tiled=False).astype(jnp.float32)
    width = gated.shape[1] // 2
    routed_hidden = (jax.nn.silu(gated[:, :width]) * gated[:, width:]).astype(jnp.bfloat16)
    shared_hidden = (
        jax.nn.silu(jnp.dot(group_normed, shared_gate, preferred_element_type=jnp.float32))
        * jnp.dot(group_normed, shared_up, preferred_element_type=jnp.float32)
    ).astype(jnp.bfloat16)
    hidden = lax.all_gather(
        jnp.concatenate([routed_hidden, shared_hidden], axis=0), "tp", axis=0, tiled=False
    )
    routed_out, shared_out = down_call(hidden, weights, slots, cols)
    expert_rows = lax.all_to_all(
        routed_out.reshape(groups, -1, cols), "sp", split_axis=0, concat_axis=0, tiled=True
    ).reshape(slots, cols)
    moe = (
        shared_out
        + jnp.dot(share_high, expert_rows, preferred_element_type=jnp.float32)
        + jnp.dot(share_low, expert_rows, preferred_element_type=jnp.float32)
    )
    moe = lax.all_to_all(
        moe.astype(jnp.bfloat16).reshape(tp_count, rows_here, cols),
        "tp",
        split_axis=0,
        concat_axis=0,
        tiled=True,
    )
    moe = moe.transpose(1, 0, 2).reshape(rows_here, MODEL_DIM).astype(jnp.float32)
    return (mixed.astype(jnp.float32) + rms_scale(moe, moe_gain)).astype(jnp.bfloat16)


def solution(mesh):
    in_specs = (
        P("sp", "tp"),
        P("sp", "tp"),
        P("sp", None),
        P("sp", None),
        P(),
        P(None, "tp"),
        P(None, "tp"),
        P("tp", None),
        P(("sp", "tp"), None),
        P(),
        P(),
        P(("sp", "tp"), None),
        P(("sp", "tp"), None),
        P("sp", None, "tp"),
        P("sp", None, "tp"),
        P("sp", "tp", None),
        P(None, "tp"),
        P(None, "tp"),
        P("tp", None),
        P(),
    )
    out_specs = P(("sp", "tp"), None)
    return jax.shard_map(layer, mesh=mesh, in_specs=in_specs, out_specs=out_specs, check_vma=False)
```

time: 661 us -> 443 us (0.67)
  blocking collectives: 302 us -> 108 us
  Pallas kernels: 0 us -> 60.8 us
  matrix products: 51.7 us -> 10.6 us
  waiting for transfers between devices: 204 us -> 173 us
  local copies, waits for them, and re-layouts: 54.2 us -> 27.5 us
  other arithmetic: 18.1 us -> 34.6 us
    all_to_all x1 -> x4, blocking collectives: 275 us -> 97 us  [the longest x1 31.3 us: layer(): lax.all_to_all(table.reshape(groups, -1, cols), 'sp', split_axis=0, conca...]
    pallas_call x0 -> x3, Pallas kernels: none -> 60.8 us  [the longest x1 51.2 us: attention_call(): pl.pallas_call(functools.partial(attention_kernel, block=rows * 2, score_...]
    all_to_all x2, waiting for transfers between devices: 50 us -> 103 us  [the longest x1 103 us: layer(): lax.all_to_all(jnp.concatenate([gate_up, downs], axis=1), 'tp', split_axi...]
    all_gather x3, waiting for transfers between devices: 80.6 us -> 32.4 us  [the longest x1 29.5 us: layer(): lax.all_gather(jnp.concatenate([routed_hidden, shared_hidden], axis=0), '...]
    reduce_scatter x2 -> x1, waiting for transfers between devices: 72.7 us -> 31.1 us  [layer(): lax.psum_scatter(partial, 'tp', scatter_dimension=0, tiled=False)]
    dot_general x11 -> x6, matrix products: 51.7 us -> 10.6 us  [the longest x1 5.23 us: layer(): lax.dot_general(attended, out_proj, (((0,), (0,)), ((), ())), preferred_e...]
    reshape x5, local copies, waits for them, and re-layouts: 28.7 us -> 0.46 us  [the longest x1 0.28 us: layer(): normed.reshape(rows_here, tp_count, cols).transpose(1, 0, 2)]
    concatenate x0 -> x8, other arithmetic: none -> 24.7 us  [the longest x1 10.4 us: layer(): jnp.concatenate([query_tiles(query_nope, query_rot), query_tiles(far_quer...]
  transfers between devices with their start and end apart: 7 -> 8, of which waited for: 5 -> 6; matrix products, arithmetic and copies ran while one was open for 12% -> 11% of each run, Pallas kernels for 0% -> 1%
where the time goes in v1:
time: 443 us; the launch traced here: 442 us
  waiting for transfers between devices  173 us (39%)
  blocking collectives  108 us (24%)
  Pallas kernels  60.8 us (14%)
  other arithmetic  34.6 us (8%)
  local copies, waits for them, and re-layouts  27.5 us (6%)
  between operations  14.8 us (3%)
  starting transfers between devices  12 us (3%)
  matrix products  10.6 us (2%)
    all_to_all x1, waiting for transfers between devices, layer(): lax.all_to_all(jnp.concatenate([gate_up, downs], axis=1), 'tp', split_axi...  103 us
    pallas_call x1, Pallas kernels, attention_call(): pl.pallas_call(functools.partial(attention_kernel, block=rows * 2, score_...  51.2 us
    all_to_all x1, blocking collectives, layer(): lax.all_to_all(table.reshape(groups, -1, cols), 'sp', split_axis=0, conca...  31.3 us
    reduce_scatter x1, waiting for transfers between devices, layer(): lax.psum_scatter(partial, 'tp', scatter_dimension=0, tiled=False)  31.1 us
    all_to_all x1, blocking collectives, layer(): lax.all_to_all(routed_out.reshape(groups, -1, cols), 'sp', split_axis=0,...  30 us
    all_gather x1, waiting for transfers between devices, layer(): lax.all_gather(jnp.concatenate([routed_hidden, shared_hidden], axis=0), '...  29.5 us
    all_to_all x1, blocking collectives, sum_at_owner(): lax.all_to_all(cut_along(array, dim, count), axis, 0, 0, tiled=True)  24.6 us
    concatenate x4, local copies, waits for them, and re-layouts, layer(): downs = jnp.concatenate([expert_down[0], shared_down], axis=0)  15 us
  transfers between devices with their start and end apart: 8, of which 6 were waited for; matrix products, arithmetic and copies ran while one was open for 11% of the time, Pallas kernels for 1%

profile of v1, /device:TPU:0, one launch (start us, length us, event | category | flops | bytes accessed | tf_op | source)
XLA Modules:
  0.0 441.8 jit_solution(10219681604131964186)
XLA Ops:
  14.5 4.5 %concatenate.86 = bf16[256,4,2,512]{3,2,1,0:T(2,128)(2,1)} reshape(bf16[256,4096]{1,0:T(8,128)(2,1)} %param.39) | data formatting | bytes 4194304 | tf_op jit(solution)/shard_map/concatenate | solution.py:350
  19.0 3.7 copy.111
  22.6 4.5 %concatenate.85 = bf16[256,4,2,512]{3,2,1,0:T(2,128)(2,1)} reshape(bf16[1,256,4096]{2,1,0:T(8,128)(2,1)} %param.36) | data formatting | bytes 4194304 | tf_op jit(solution)/shard_map/concatenate | solution.py:350
  27.1 2.4 copy.110
  29.6 11.3 %all-gather.3 = f32[4,48,4]{1,2,0:T(4,128)S(1)} all-gather(f32[1,48,4]{1,2,0:T(4,128)S(1)} %maximum_bitcast_fusion.1), channel_id=2, replica_groups=mesh['sp'=32,'tp'=4] {'tp'}, dimensions={0}, use_global_device_ids=true | all-gather | bytes 3840 | tf_op jit(solution)/shard_map/all_gather | solution.py:344
  40.9 2.4 pad_maximum_fusion.1
  43.3 2.2 pad_maximum_fusion.2
  53.0 10.4 %fusion.17.qt_ref = bf16[12,256,384]{2,1,0:T(8,128)(2,1)} fusion(bf16[4,64,192]{2,1,0:T(8,128)(2,1)S(1)} %get-tuple-element.36, bf16[4,64,192]{2,1,0:T(8,128)(2,1)S(1)} %get-tuple-element.35, bf16[8,64,192]{2,1,0:T(8,128)(2,1)S(1)} %get-tuple-element.32, bf16[8,64,192]{2,1,0:T(8,128)(2,1)S(1)} %get-tuple-element.31, ...), kind=kLoop, calls=%fused_computation.27 | loop fusion | flops 46006272 | bytes 3256320 | tf_op jit(solution)/shard_map/concatenate | solution.py:366
  63.5 2.8 all-gather.10.cloned.1.call-done
  67.5 51.2 %shard_map.199 = bf16[12,128,192]{2,1,0:T(8,128)(2,1)S(1)} custom-call(s32[4]{0:T(128)S(1)} %pad_add_fusion.desc_ref, bf16[32,208,512]{2,1,0:T(8,128)(2,1)} %bitcast.116, bf16[12,256,384]{2,1,0:T(8,128)(2,1)} %fusion.17.qt_ref, bf16[512,1024]{1,0:T(8,128)(2,1)S(1)} %copy-done.3, bf16[512,1024]{1,0:T(8,128)(2,1)S(1)} %copy-done.4), custom_call_target="tpu_custom_call" | custom-call | flops 49999998976 | bytes 12000000 | tf_op jit(solution)/shard_map/pallas_call | solution.py:251
  120.0 6.2 %collective-permute-done.1 = bf16[4,128,192]{2,1,0:T(8,128)(2,1)S(1)} collective-permute-done((bf16[4,128,192]{2,1,0:T(8,128)(2,1)S(1)}, bf16[4,128,192]{2,1,0:T(8,128)(2,1)S(1)}, u32[]{:S(2)}, u32[]{:S(2)}) %collective-permute-start.1) | collective-permute-done | bytes 196640 | tf_op jit(solution)/shard_map/ppermute | solution.py:379
  126.4 5.2 %convolution_convert_fusion = bf16[192,4096]{1,0:T(8,128)(2,1)S(1)} fusion(bf16[1024,192]{1,0:T(8,128)(2,1)S(1)} %bitcast.95, bf16[1024,4096]{1,0:T(8,128)(2,1)} %param.28), kind=kOutput, calls=%fused_computation.7 | convolution fusion | flops 1611399168 | bytes 10354688 | tf_op jit(solution)/shard_map/dot_general | solution.py:388
  131.7 24.6 %all_to_all.30 = bf16[4,48,4096]{2,1,0:T(8,128)(2,1)S(1)} all-to-all(bf16[4,48,4096]{2,1,0:T(8,128)(2,1)S(1)} %bitcast.94), channel_id=1, replica_groups=mesh['sp'=32,'tp'=4] {'tp'}, dimensions={0} | all-to-all | bytes 3145728 | tf_op jit(solution)/shard_map/all_to_all | solution.py:29
  159.0 3.5 all-to-all-start.1
  162.4 7.2 %pad_maximum_fusion = bf16[4,2048,512]{2,1,0:T(8,128)(2,1)} fusion(bf16[4,1024,512]{2,1,0:T(8,128)(2,1)} %bitcast.90, bf16[4,1024,512]{2,1,0:T(8,128)(2,1)} %pad_maximum_fusion.1), kind=kLoop, calls=%fused_computation | loop fusion | flops 16777216 | bytes 16777216 | tf_op jit(solution)/shard_map/concatenate | solution.py:355
  169.8 5.8 %all-to-all-start.3 = ((bf16[4,2048,512]{2,1,0:T(8,128)(2,1)}), bf16[4,2048,512]{2,1,0:T(8,128)(2,1)}, u32[]{:S(2)}, u32[]{:S(2)}) async-start(bf16[4,2048,512]{2,1,0:T(8,128)(2,1)} %pad_maximum_fusion), calls=%async_computation.3 | async-start | bytes 16777216 | tf_op jit(solution)/shard_map/all_to_all | solution.py:354
  178.1 102.8 %all-to-all-done.3.w_ref = bf16[4,2048,512]{2,1,0:T(8,128)(2,1)} async-done(((bf16[4,2048,512]{2,1,0:T(8,128)(2,1)}), bf16[4,2048,512]{2,1,0:T(8,128)(2,1)}, u32[]{:S(2)}, u32[]{:S(2)}) %all-to-all-start.3) | async-done | bytes 8388640 | tf_op jit(solution)/shard_map/all_to_all | solution.py:354
  280.9 31.3 %all_to_all.31 = bf16[32,24,1024]{2,1,0:T(8,128)(2,1)S(1)} all-to-all(bf16[32,24,1024]{2,1,0:T(8,128)(2,1)} %bitcast.93), channel_id=1, replica_groups=mesh['sp'=32,'tp'=4] {'sp'}, dimensions={0} | all-to-all | bytes 3145728 | tf_op jit(solution)/shard_map/all_to_all | solution.py:405
  312.1 5.5 %shard_map.200 = bf16[4,768,512]{2,1,0:T(8,128)(2,1)S(1)} custom-call(bf16[768,1024]{1,0:T(8,128)(2,1)S(1)} %bitcast.87, bf16[4,2048,512]{2,1,0:T(8,128)(2,1)} %all-to-all-done.3.w_ref), custom_call_target="tpu_custom_call" | custom-call | flops 3221225472 | bytes 9000000 | tf_op jit(solution)/shard_map/pallas_call | solution.py:67
  322.6 31.1 %reduce-scatter.2.cloned.1.call-done = bf16[1,768,512]{2,1,0:T(8,128)(2,1)} async-done(((bf16[4,768,512]{2,1,0:T(8,128)(2,1)}), bf16[1,768,512]{2,1,0:T(8,128)(2,1)}) %reduce-scatter.2.cloned.1.call-update) | async-done | bytes 786448 | tf_op jit(solution)/shard_map/reduce_scatter | solution.py:409
  356.1 29.5 %all-gather.12.cloned.1.call-done = bf16[3840,256]{1,0:T(8,128)(2,1)} async-done(((bf16[960,256]{1,0:T(8,128)(2,1)}), bf16[3840,256]{1,0:T(8,128)(2,1)}) %all-gather.12.cloned.1.call-update) | async-done | bytes 1966096 | tf_op jit(solution)/shard_map/all_gather | solution.py:416
  387.2 4.1 shard_map.201
  391.4 30.0 %all_to_all.32 = bf16[32,24,1024]{2,1,0:T(8,128)(2,1)S(1)} all-to-all(bf16[32,24,1024]{2,1,0:T(8,128)(2,1)S(1)} %bitcast.89), channel_id=1, replica_groups=mesh['sp'=32,'tp'=4] {'sp'}, dimensions={0} | all-to-all | bytes 3145728 | tf_op jit(solution)/shard_map/all_to_all | solution.py:420
  422.9 11.1 %all_to_all.33 = bf16[4,48,1024]{2,1,0:T(8,128)(2,1)S(1)} all-to-all(bf16[4,48,1024]{2,1,0:T(8,128)(2,1)S(1)} %bitcast.101), channel_id=1, replica_groups=mesh['sp'=32,'tp'=4] {'tp'}, dimensions={0} | all-to-all | bytes 786432 | tf_op jit(solution)/shard_map/all_to_all | solution.py:428
  (143 shorter events, 33.8 us)
Async XLA Ops:
  6.5 313.0 %copy-start = (bf16[4096,256]{1,0:T(8,128)(2,1)S(1)}, bf16[4096,256]{1,0:T(8,128)(2,1)}, u32[]{:S(2)}) copy-start(bf16[4096,256]{1,0:T(8,128)(2,1)} %param.37) | copy-start | bytes 6291460
  6.5 5.6 %copy-start.13 = (bf16[192,1024]{1,0:T(8,128)(2,1)S(1)}, bf16[192,1024]{1,0:T(8,128)(2,1)}, u32[]{:S(2)}) copy-start(bf16[192,1024]{1,0:T(8,128)(2,1)} %param.21) | copy-start | bytes 1179652
  6.5 59.7 %all-gather.10.cloned.1.call-start = ((), (), s32[]{:S(2)}) async-start(), calls=%async_computation.9 | async-start | bytes 7028736 | tf_op jit(solution)/shard_map/all_gather | solution.py:340
  13.2 37.8 %collective-permute-start = (bf16[192,768]{0,1:T(8,128)(2,1)}, bf16[192,768]{0,1:T(8,128)(2,1)}, u32[]{:S(2)}, u32[]{:S(2)}) collective-permute-start(bf16[192,768]{0,1:T(8,128)(2,1)} %pad_maximum_fusion.5), channel_id=1, source_target_pairs={{124,0},{120,4},{116,8},{112,12},{108,16},{104,20},{100,24},{96,28... | collective-permute-start | bytes 884744 | tf_op jit(solution)/shard_map/ppermute | solution.py:335
  22.6 6.9 %copy-start.18 = (s32[48,2]{0,1:T(2,128)S(1)}, s32[48,2]{0,1:T(2,128)}, u32[]{:S(2)}) copy-start(s32[48,2]{0,1:T(2,128)} %param.32) | copy-start | bytes 1156
  27.1 2.5 copy-start.19
  27.1 13.7 %copy-start.8 = (bf16[1,4096,256]{2,1,0:T(8,128)(2,1)S(1)}, bf16[1,4096,256]{2,1,0:T(8,128)(2,1)}, u32[]{:S(2)}) copy-start(bf16[1,4096,256]{2,1,0:T(8,128)(2,1)} %param.35) | copy-start | bytes 6291460
  27.1 13.8 %copy-start.9 = (bf16[1,4096,256]{2,1,0:T(8,128)(2,1)S(1)}, bf16[1,4096,256]{2,1,0:T(8,128)(2,1)}, u32[]{:S(2)}) copy-start(bf16[1,4096,256]{2,1,0:T(8,128)(2,1)} %param.34) | copy-start | bytes 6291460
  40.9 2.4 copy-start.5
  43.3 2.2 copy-start.21
  52.9 13.3 %copy-start.3 = (bf16[512,1024]{1,0:T(8,128)(2,1)S(1)}, bf16[512,1024]{1,0:T(8,128)(2,1)}, u32[]{:S(2)}) copy-start(bf16[512,1024]{1,0:T(8,128)(2,1)} %ku_ref.1) | copy-start | bytes 3145732
  118.7 7.5 %collective-permute-start.1 = (bf16[4,128,192]{2,1,0:T(8,128)(2,1)S(1)}, bf16[4,128,192]{2,1,0:T(8,128)(2,1)S(1)}, u32[]{:S(2)}, u32[]{:S(2)}) collective-permute-start(bf16[4,128,192]{2,1,0:T(8,128)(2,1)S(1)} %get-tuple-element.26), channel_id=1, source_target_pairs={{0,124},{4,120},{8,116},{12,112},{16,108},{20,104},{24,100},{28,96... | collective-permute-start | bytes 589832 | tf_op jit(solution)/shard_map/ppermute | solution.py:379
  157.8 11.9 %copy-start.6 = (bf16[48,4096]{1,0:T(8,128)(2,1)}, bf16[48,4096]{1,0:T(8,128)(2,1)S(1)}, u32[]{:S(2)}) copy-start(bf16[48,4096]{1,0:T(8,128)(2,1)S(1)} %fusion.27) | copy-start | bytes 1179652
  159.0 10.8 %all-to-all-start.1 = ((bf16[4,48,1024]{2,1,0:T(8,128)(2,1)}), bf16[4,48,1024]{2,1,0:T(8,128)(2,1)S(1)}, u32[]{:S(2)}, u32[]{:S(2)}) async-start(bf16[4,48,1024]{2,1,0:T(8,128)(2,1)} %copy.128), calls=%async_computation.1 | async-start | bytes 786432 | tf_op jit(solution)/shard_map/all_to_all | solution.py:395
  169.8 6.6 %copy-start.10 = (bf16[768,192]{0,1:T(8,128)(2,1)S(1)}, bf16[768,192]{0,1:T(8,128)(2,1)}, u32[]{:S(2)}) copy-start(bf16[768,192]{0,1:T(8,128)(2,1)} %convert_element_type.109) | copy-start | bytes 884740
  169.8 111.1 %all-to-all-start.3 = ((bf16[4,2048,512]{2,1,0:T(8,128)(2,1)}), bf16[4,2048,512]{2,1,0:T(8,128)(2,1)}, u32[]{:S(2)}, u32[]{:S(2)}) async-start(bf16[4,2048,512]{2,1,0:T(8,128)(2,1)} %pad_maximum_fusion), calls=%async_computation.3 | async-start | bytes 16777216 | tf_op jit(solution)/shard_map/all_to_all | solution.py:354
  175.6 143.9 %all-gather.8.cloned.1.call-start = ((), (), s32[]{:S(2)}) async-start(), calls=%async_computation.8 | async-start | bytes 1966080 | tf_op jit(solution)/shard_map/all_gather | solution.py:402
  176.3 177.4 %reduce-scatter.2.cloned.1.call-start = ((), (), s32[]{:S(2)}) async-start(), calls=%async_computation.7 | async-start | bytes 3932160 | tf_op jit(solution)/shard_map/reduce_scatter | solution.py:409
  317.6 1.8 copy-start.1
  319.4 66.3 %all-gather.12.cloned.1.call-start = ((), (), s32[]{:S(2)}) async-start(), calls=%async_computation.10 | async-start | bytes 2457600 | tf_op jit(solution)/shard_map/all_gather | solution.py:416
  319.5 2.2 copy-start.7
  319.5 2.5 copy-start.20
  391.4 30.0 %copy-start.12 = (bf16[192,768]{1,0:T(8,128)(2,1)S(1)}, bf16[192,768]{1,0:T(8,128)(2,1)}, u32[]{:S(2)}) copy-start(bf16[192,768]{1,0:T(8,128)(2,1)} %get-tuple-element.20) | copy-start | bytes 884740
  422.8 11.5 %copy-start.16 = (f32[4096]{0:T(1024)S(1)}, f32[4096]{0:T(1024)}, u32[]{:S(2)}) copy-start(f32[4096]{0:T(1024)} %param.40) | copy-start | bytes 49156
  (6 other events, 7.1 us)
Sparse Core Ops, SparseCore 0:
  11.0 55.2 all-gather.9
  178.0 41.9 all-gather.7
  319.5 34.1 reduce-scatter.1
  356.3 29.3 all-gather.11

commit v2 on v1

--- a/solution.py
+++ b/solution.py
@@ -11,7 +11,6 @@
 MODEL_DIM = 4096
 NOPE_DIM = 64
 ROPE_DIM = 32
-VALUE_DIM = 64
 TOP_K = 2
 
 
@@ -55,6 +54,75 @@
     )
 
 
+def project_kernel(own_ref, attended_ref, returned_ref, w_ref, out_ref, x_ref):
+    pairs = x_ref.shape[1] // 128
+    kept = pairs - returned_ref.shape[0]
+
+    @pl.when(pl.program_id(0) == 0)
+    def _():
+        for pair in range(pairs):
+            x = attended_ref[pair]
+            if pair >= kept:
+                x = jnp.where(pair < own_ref[0], x, returned_ref[pair - kept])
+            x_ref[:, pair * 128 : (pair + 1) * 128] = x.astype(jnp.float32).T.astype(jnp.bfloat16)
+
+    out_ref[...] = jnp.dot(x_ref[...], w_ref[...], preferred_element_type=jnp.float32).astype(
+        out_ref.dtype
+    )
+
+
+def project_call(own, attended, returned, weights):
+    depth, cols = weights.shape
+    rows = attended.shape[2]
+    tile = cols // 8
+    return pl.pallas_call(
+        project_kernel,
+        grid=(cols // tile,),
+        out_shape=jax.ShapeDtypeStruct((rows, cols), jnp.bfloat16),
+        in_specs=[
+            pl.BlockSpec(memory_space=pltpu.SMEM),
+            pl.BlockSpec(attended.shape, lambda n: (0, 0, 0)),
+            pl.BlockSpec(returned.shape, lambda n: (0, 0, 0)),
+            pl.BlockSpec((depth, tile), lambda n: (0, n)),
+        ],
+        out_specs=pl.BlockSpec((rows, tile), lambda n: (0, n)),
+        scratch_shapes=[pltpu.VMEM((rows, depth), jnp.bfloat16)],
+        compiler_params=pltpu.CompilerParams(vmem_limit_bytes=20 * 1024 * 1024),
+        cost_estimate=pl.CostEstimate(
+            flops=2 * rows * depth * cols, bytes_accessed=11_000_000, transcendentals=0
+        ),
+    )(own, attended, returned, weights)
+
+
+def pack_kernel(gate_ref, up_ref, down_ref, out_ref):
+    cols, width = gate_ref.shape[1], gate_ref.shape[2]
+    depth, tile = down_ref.shape[1], out_ref.shape[2]
+    out_ref[0, 0:cols, 0:width] = gate_ref[0]
+    out_ref[0, 0:cols, width : 2 * width] = up_ref[0]
+    for half in range(cols // tile):
+        row = cols + half * depth
+        out_ref[0, row : row + depth] = down_ref[0, :, half * tile : (half + 1) * tile]
+
+
+def pack_call(gate, up, down, quarters):
+    cols = gate.shape[1] // quarters
+    width, depth = gate.shape[2], down.shape[1]
+    rows = cols + depth * cols // (2 * width)
+    return pl.pallas_call(
+        pack_kernel,
+        grid=(quarters,),
+        out_shape=jax.ShapeDtypeStruct((quarters, rows, 2 * width), gate.dtype),
+        in_specs=[
+            pl.BlockSpec((1, cols, width), lambda q: (0, q, 0)),
+            pl.BlockSpec((1, cols, width), lambda q: (0, q, 0)),
+            pl.BlockSpec((1, depth, cols), lambda q: (0, 0, q)),
+        ],
+        out_specs=pl.BlockSpec((1, rows, 2 * width), lambda q: (q, 0, 0)),
+        compiler_params=pltpu.CompilerParams(vmem_limit_bytes=56 * 1024 * 1024),
+        cost_estimate=pl.CostEstimate(flops=0, bytes_accessed=13_000_000, transcendentals=0),
+    )(gate, up, down)
+
+
 def gate_kernel(x_ref, w_ref, out_ref):
     out_ref[0] = jnp.dot(x_ref[...], w_ref[0], preferred_element_type=jnp.float32).astype(
         out_ref.dtype
@@ -73,53 +141,44 @@
             pl.BlockSpec((1, depth, width), lambda q: (q, 0, 0)),
         ],
         out_specs=pl.BlockSpec((1, rows, width), lambda q: (q, 0, 0)),
-        compiler_params=pltpu.CompilerParams(vmem_limit_bytes=40 * 1024 * 1024),
+        compiler_params=pltpu.CompilerParams(vmem_limit_bytes=56 * 1024 * 1024),
         cost_estimate=pl.CostEstimate(
             flops=2 * rows * depth * width * quarters, bytes_accessed=9_000_000, transcendentals=0
         ),
     )(x, weights)
 
 
-def down_kernel(hidden_ref, w_ref, routed_ref, shared_ref):
-    quarters = hidden_ref.shape[0]
-    half = w_ref.shape[1] // 2
-    routed_rows = routed_ref.shape[0]
-    routed = shared = 0.0
-    for q in range(quarters):
-        routed += jnp.dot(
-            hidden_ref[q, :routed_rows], w_ref[q, :half], preferred_element_type=jnp.float32
+def down_kernel(first_ref, second_ref, w_ref, routed_ref):
+    quarters, middle, _ = first_ref.shape
+
+    def total(ref):
+        return sum(
+            jnp.dot(ref[q], w_ref[q], preferred_element_type=jnp.float32) for q in range(quarters)
         )
-        shared += jnp.dot(
-            hidden_ref[q, routed_rows:], w_ref[q, half:], preferred_element_type=jnp.float32
-        )
-    routed_ref[...] = routed.astype(routed_ref.dtype)
-    shared_ref[...] = shared
-
-
-def down_call(hidden, weights, routed_rows, cols):
-    quarters, rows, half = hidden.shape
+
+    routed_ref[:middle] = total(first_ref).astype(routed_ref.dtype)
+    routed_ref[middle:] = total(second_ref).astype(routed_ref.dtype)
+
+
+def down_call(first_half, second_half, weights, cols):
+    quarters, middle, half = first_half.shape
     tile = weights.shape[2]
-    first = (weights.shape[1] - 2 * half * cols // tile) // (2 * half)
+    first = weights.shape[1] // half - cols // tile
     return pl.pallas_call(
         down_kernel,
         grid=(cols // tile,),
-        out_shape=(
-            jax.ShapeDtypeStruct((routed_rows, cols), jnp.bfloat16),
-            jax.ShapeDtypeStruct((rows - routed_rows, cols), jnp.float32),
+        out_shape=jax.ShapeDtypeStruct((2 * middle, cols), jnp.bfloat16),
+        in_specs=[
+            pl.BlockSpec((quarters, middle, half), lambda n: (0, 0, 0)),
+            pl.BlockSpec((quarters, middle, half), lambda n: (0, 0, 0)),
+            pl.BlockSpec((quarters, half, tile), lambda n: (0, first + n, 0)),
+        ],
+        out_specs=pl.BlockSpec((2 * middle, tile), lambda n: (0, n)),
+        compiler_params=pltpu.CompilerParams(vmem_limit_bytes=24 * 1024 * 1024),
+        cost_estimate=pl.CostEstimate(
+            flops=4 * middle * half * quarters * cols, bytes_accessed=8_000_000, transcendentals=0
         ),
-        in_specs=[
-            pl.BlockSpec((quarters, rows, half), lambda n: (0, 0, 0)),
-            pl.BlockSpec((quarters, 2 * half, tile), lambda n: (0, first + n, 0)),
-        ],
-        out_specs=(
-            pl.BlockSpec((routed_rows, tile), lambda n: (0, n)),
-            pl.BlockSpec((rows - routed_rows, tile), lambda n: (0, n)),
-        ),
-        compiler_params=pltpu.CompilerParams(vmem_limit_bytes=40 * 1024 * 1024),
-        cost_estimate=pl.CostEstimate(
-            flops=2 * rows * half * quarters * cols, bytes_accessed=8_000_000, transcendentals=0
-        ),
-    )(hidden, weights)
+    )(first_half, second_half, weights)
 
 
 def slot_tables(routes, weights, experts, capacity):
@@ -147,7 +206,7 @@
 def far_pairs(groups, pairs):
     counts = []
     for low in range(groups // 2):
-        mine, theirs = low // 2 + 2.1, (groups - 1 - low) // 2 + 2.1
+        mine, theirs = low + 5.6, groups + 4.6 - low
         best = min(
             range(pairs // 2 + 1),
             key=lambda n: max(pairs * mine + n * theirs, (pairs - n) * theirs),
@@ -158,6 +217,8 @@
 
 LOG2E = 1.4426950408889634
 PACK_ROWS = 16
+CHAINS = (10, 5, 2, 1)
+ATTEND_VMEM = 44
 
 
 def attention_kernel(
@@ -193,13 +254,23 @@
         w_ref[:, 0:128] = ku_ref[:, pl.ds(col, 128)]
         w_ref[:, 128:256] = vu_ref[:, pl.ds(col, 128)]
 
+        count_all = index + 1
+        row = lax.broadcasted_iota(jnp.int32, (block, width), 0)
+        lane = lax.broadcasted_iota(jnp.int32, (block, width), 1)
+        ahead = row - jnp.where(lane >= half, lane - half, lane) - index * rows
+        state = (
+            jnp.full((1, width), -1e30, jnp.float32),
+            jnp.zeros((1, width), jnp.float32),
+            jnp.zeros((128, width), jnp.float32),
+        )
+
         def scores(b):
             lat = gath_ref[pl.ds(b * per, per), 0:rows, :].reshape(block, lat_dim)
             kv = jnp.dot(lat, w_ref[...], preferred_element_type=jnp.float32).astype(jnp.bfloat16)
             rot = rot_ref[pl.ds(b * per, per)].reshape(block, 128)
             keys = jnp.concatenate([kv[:, :128], rot], axis=1)
             s = jnp.dot(keys, qt_ref[slot], preferred_element_type=jnp.float32)
-            return s, kv[:, 128:]
+            return jnp.where(ahead <= -b * block, s, -1e30), kv[:, 128:]
 
         def weigh(v, p):
             return lax.dot_general(
@@ -209,16 +280,6 @@
                 preferred_element_type=jnp.float32,
             )
 
-        full = (index * rows) // block
-        s, v = scores(full)
-        key = lax.broadcasted_iota(jnp.int32, (block, width), 0) + full * block
-        lane = lax.broadcasted_iota(jnp.int32, (block, width), 1)
-        query = index * rows + jnp.where(lane >= half, lane - half, lane)
-        s = jnp.where(key <= query, s, -1e30)
-        top = jnp.max(s, axis=0, keepdims=True)
-        p = jnp.exp2(s * factor - top * factor)
-        state = (top, jnp.sum(p, axis=0, keepdims=True), weigh(v, p))
-
         def update(state, s, v):
             top, total, acc = state
             newest = jnp.maximum(top, jnp.max(s, axis=0, keepdims=True))
@@ -227,15 +288,21 @@
             total = total * alpha + jnp.sum(p, axis=0, keepdims=True)
             return newest, total, acc * alpha + weigh(v, p)
 
-        def two(b, state):
-            first, second = scores(b * 2), scores(b * 2 + 1)
-            return update(update(state, *first), *second)
-
-        state = lax.fori_loop(0, full // 2, two, state)
-        state = lax.fori_loop(
-            (full // 2) * 2, full, lambda b, state: update(state, *scores(b)), state
-        )
-        top, total, acc = state
+        def several(count):
+            def body(_, carry):
+                start, state = carry
+                found = [scores(start + k) for k in range(count)]
+                for pair_scores in found:
+                    state = update(state, *pair_scores)
+                return start + count, state
+
+            return body
+
+        carry, left = (jnp.int32(0), state), count_all
+        for count in CHAINS:
+            carry = lax.fori_loop(0, left // count, several(count), carry)
+            left = left % count
+        _, total, acc = carry[1]
         res = acc / total
         out_ref[slot, 0:64, :] = res[0:64, 0:half].astype(jnp.bfloat16)
         out_ref[slot, 64:128, :] = res[64:128, half:].astype(jnp.bfloat16)
@@ -249,7 +316,7 @@
     rows = grows - PACK_ROWS
     slots, _, width = qt.shape
     return pl.pallas_call(
-        functools.partial(attention_kernel, block=rows * 2, score_scale=score_scale),
+        functools.partial(attention_kernel, block=rows, score_scale=score_scale),
         out_shape=jax.ShapeDtypeStruct((slots, 128, width // 2), jnp.bfloat16),
         in_specs=[pl.BlockSpec(memory_space=pltpu.SMEM)]
         + [pl.BlockSpec(memory_space=pltpu.VMEM)] * 4,
@@ -258,7 +325,7 @@
             pltpu.VMEM((devices, rows, 128), jnp.bfloat16),
             pltpu.VMEM((lat_dim, 256), jnp.bfloat16),
         ],
-        compiler_params=pltpu.CompilerParams(vmem_limit_bytes=50 * 1024 * 1024),
+        compiler_params=pltpu.CompilerParams(vmem_limit_bytes=ATTEND_VMEM * 1024 * 1024),
         cost_estimate=pl.CostEstimate(
             flops=50_000_000_000, bytes_accessed=12_000_000, transcendentals=20_000_000
         ),
@@ -318,7 +385,8 @@
     place = lax.axis_index("sp").astype(jnp.int32)
     tp_count = lax.axis_size("tp")
     pairs = heads_here // 2
-    far = pairs // 2
+    counts = far_pairs(groups, pairs)
+    far = max(1, max(counts))
     cols = MODEL_DIM // tp_count
     rows_here = resid.shape[0]
     capacity = max(2, 2 * rows_here * TOP_K // groups)
@@ -326,8 +394,8 @@
 
     sent_queries = jnp.concatenate(
         [
-            query_nope[:, far * 2 * NOPE_DIM :],
-            query_rot.reshape(local_rows, -1)[:, far * 2 * ROPE_DIM :],
+            query_nope[:, (pairs - far) * 2 * NOPE_DIM :],
+            query_rot.reshape(local_rows, -1)[:, (pairs - far) * 2 * ROPE_DIM :],
         ],
         axis=1,
     )
@@ -341,26 +409,25 @@
         jnp.concatenate([latent_normed, packed_rot], axis=0), "sp", axis=0, tiled=False
     )
 
-    route_data = lax.all_gather(
-        jnp.concatenate([routes.astype(jnp.float32), route_weights], axis=1), "tp", axis=0
-    )
-    gate_up = jnp.concatenate([expert_gate[0], expert_up[0]], axis=1)
-    gate_width = gate_up.shape[1]
-    gate_up = gate_up.reshape(tp_count, cols, gate_width)
-    downs = jnp.concatenate([expert_down[0], shared_down], axis=0)
-    downs = downs.reshape(downs.shape[0], tp_count, cols // gate_width, gate_width)
-    downs = downs.transpose(1, 2, 0, 3).reshape(tp_count, -1, gate_width)
-    gate_up, downs, route_data = lax.optimization_barrier((gate_up, downs, route_data))
-    weights = lax.all_to_all(
-        jnp.concatenate([gate_up, downs], axis=1), "tp", split_axis=0, concat_axis=0, tiled=True
-    )
+    own_routes = jnp.concatenate([routes.astype(jnp.float32), route_weights], axis=1)
+    turn = lax.axis_index("tp")
+    parts = [own_routes] + [
+        lax.ppermute(own_routes, "tp", [(d, (d + k) % tp_count) for d in range(tp_count)])
+        for k in range(1, tp_count)
+    ]
+    owner = jnp.arange(tp_count, dtype=jnp.int32)[:, None, None]
+    route_data = sum(
+        jnp.where(owner == (turn - k) % tp_count, part[None], 0.0) for k, part in enumerate(parts)
+    )
+    packed = pack_call(expert_gate, expert_up, expert_down, tp_count)
+    weights = lax.all_to_all(packed, "tp", split_axis=0, concat_axis=0, tiled=True)
     spread, share_high, share_low = slot_tables(
         route_data[..., :TOP_K].astype(jnp.int32), route_data[..., TOP_K:], groups, capacity
     )
 
     is_low = place < groups // 2
     low_place = jnp.minimum(place, groups - 1 - place)
-    moved = jnp.asarray(far_pairs(groups, pairs), jnp.int32)[low_place]
+    moved = jnp.asarray(counts, jnp.int32)[low_place]
     n_own = jnp.where(is_low, pairs, pairs - moved)
     desc = jnp.stack([n_own, place, jnp.where(is_low, moved, 0), groups - 1 - place])
     tiles = jnp.concatenate(
@@ -377,23 +444,13 @@
     )
     attended = attention_call(desc, gathered, tiles, key_up, value_up, score_scale)
     returned = lax.ppermute(attended[pairs:], "sp", [(low, high) for high, low in down_pairs])
-    pair_ids = jnp.arange(pairs - far, pairs, dtype=jnp.int32)[:, None, None]
-    attended = jnp.concatenate(
-        [
-            attended[: pairs - far],
-            jnp.where(pair_ids < n_own, attended[pairs - far : pairs], returned),
-        ],
-        axis=0,
-    ).reshape(heads_here * VALUE_DIM, local_rows)
-    partial = lax.dot_general(
-        attended, out_proj, (((0,), (0,)), ((), ())), preferred_element_type=jnp.float32
-    ).astype(jnp.bfloat16)
+    partial = project_call(n_own.reshape(1), attended, returned, out_proj)
     projected = sum_at_owner(partial, "tp", 0)
     mixed = (resid.astype(jnp.float32) + rms_scale(projected, attn_gain)).astype(jnp.bfloat16)
     normed = rms_scale(mixed.astype(jnp.float32), pre_gain).astype(jnp.bfloat16)
 
     columns = lax.all_to_all(
-        normed.reshape(rows_here, tp_count, cols).transpose(1, 0, 2),
+        jnp.stack([normed[:, q * cols : (q + 1) * cols] for q in range(tp_count)]),
         "tp",
         split_axis=0,
         concat_axis=0,
@@ -406,24 +463,30 @@
         table.reshape(groups, -1, cols), "sp", split_axis=0, concat_axis=0, tiled=True
     ).reshape(slots, cols)
     partial = gate_call(arrived, weights)
-    gated = lax.psum_scatter(partial, "tp", scatter_dimension=0, tiled=False).astype(jnp.float32)
+    partial, group_normed = lax.optimization_barrier((partial, group_normed))
+    gated = lax.psum_scatter(partial, "tp", scatter_dimension=0, tiled=False)
+    gated = gated.astype(jnp.float32)
     width = gated.shape[1] // 2
     routed_hidden = (jax.nn.silu(gated[:, :width]) * gated[:, width:]).astype(jnp.bfloat16)
     shared_hidden = (
         jax.nn.silu(jnp.dot(group_normed, shared_gate, preferred_element_type=jnp.float32))
         * jnp.dot(group_normed, shared_up, preferred_element_type=jnp.float32)
     ).astype(jnp.bfloat16)
-    hidden = lax.all_gather(
-        jnp.concatenate([routed_hidden, shared_hidden], axis=0), "tp", axis=0, tiled=False
-    )
-    routed_out, shared_out = down_call(hidden, weights, slots, cols)
+    shared_part = jnp.dot(shared_hidden, shared_down, preferred_element_type=jnp.float32)
+    shared_part = shared_part.astype(jnp.bfloat16).reshape(tp_count, rows_here, MODEL_DIM)
+    middle = slots // 2
+    hidden = [
+        lax.all_gather(piece, "tp", axis=0, tiled=False)
+        for piece in (routed_hidden[:middle], routed_hidden[middle:])
+    ]
+    routed_out = down_call(*hidden, weights, cols)
+    routed_out, shared_part = lax.optimization_barrier((routed_out, shared_part))
+    shared_out = lax.psum_scatter(shared_part, "tp", scatter_dimension=0, tiled=False)
     expert_rows = lax.all_to_all(
         routed_out.reshape(groups, -1, cols), "sp", split_axis=0, concat_axis=0, tiled=True
     ).reshape(slots, cols)
-    moe = (
-        shared_out
-        + jnp.dot(share_high, expert_rows, preferred_element_type=jnp.float32)
-        + jnp.dot(share_low, expert_rows, preferred_element_type=jnp.float32)
+    moe = jnp.dot(share_high, expert_rows, preferred_element_type=jnp.float32) + jnp.dot(
+        share_low, expert_rows, preferred_element_type=jnp.float32
     )
     moe = lax.all_to_all(
         moe.astype(jnp.bfloat16).reshape(tp_count, rows_here, cols),
@@ -432,7 +495,8 @@
         concat_axis=0,
         tiled=True,
     )
-    moe = moe.transpose(1, 0, 2).reshape(rows_here, MODEL_DIM).astype(jnp.float32)
+    moe = jnp.concatenate([moe[q] for q in range(tp_count)], axis=1).astype(jnp.float32)
+    moe = moe + shared_out.astype(jnp.float32)
     return (mixed.astype(jnp.float32) + rms_scale(moe, moe_gain)).astype(jnp.bfloat16)
 
 

time: 443 us -> 406 us (0.916)
  waiting for transfers between devices: 173 us -> 139 us
  blocking collectives: 108 us -> 126 us
  starting transfers between devices: 12 us -> 26.9 us
  local copies, waits for them, and re-layouts: 27.5 us -> 12.7 us
  other arithmetic: 34.6 us -> 22.4 us
  Pallas kernels: 60.8 us -> 52 us
    all_gather x1 -> x0, waiting for transfers between devices: 29.5 us -> none  [layer(): lax.all_gather(jnp.concatenate([routed_hidden, shared_hidden], axis=0), '...]
    all_to_all x2, waiting for transfers between devices: 103 us -> 80 us  [the longest x1 78.5 us: layer(): lax.all_to_all(packed, 'tp', split_axis=0, concat_axis=0, tiled=True)]
    all_gather x1, waiting for transfers between devices: 2.82 us -> 21.2 us  [layer(): lax.all_gather(jnp.concatenate([latent_normed, packed_rot], axis=0), 'sp'...]
    all_gather x1 -> x2, blocking collectives: 11.3 us -> 28.2 us  [layer(): lax.all_gather(piece, 'tp', axis=0, tiled=False)]
    concatenate x4 -> x0, local copies, waits for them, and re-layouts: 15 us -> none  [layer(): downs = jnp.concatenate([expert_down[0], shared_down], axis=0)]
    concatenate x6 -> x2, other arithmetic: 13.6 us -> 1.44 us  [the longest x1 0.76 us: layer(): jnp.concatenate([query_nope[:, (pairs - far) * 2 * NOPE_DIM:], query_rot....]
    pallas_call x2 -> x4, Pallas kernels: 55.3 us -> 44.8 us  [the longest x1 31.6 us: attention_call(): pl.pallas_call(functools.partial(attention_kernel, block=rows, score_scal...]
    ppermute x1, starting transfers between devices: 1.31 us -> 10.7 us  [layer(): lax.ppermute(attended[pairs:], 'sp', [(low, high) for high, low in down_p...]
  transfers between devices with their start and end apart: 8 -> 11, of which waited for: 6 -> 6; matrix products, arithmetic and copies ran while one was open for 11% -> 7% of each run, Pallas kernels for 1% -> 3%
where the time goes in v2:
time: 406 us; the launch traced here: 405 us
  waiting for transfers between devices  139 us (34%)
  blocking collectives  126 us (31%)
  Pallas kernels  52 us (13%)
  starting transfers between devices  26.9 us (7%)
  other arithmetic  22.4 us (6%)
  between operations  14.8 us (4%)
  local copies, waits for them, and re-layouts  12.7 us (3%)
  matrix products  10.5 us (3%)
    all_to_all x1, waiting for transfers between devices, layer(): lax.all_to_all(packed, 'tp', split_axis=0, concat_axis=0, tiled=True)  78.5 us
    all_to_all x1, blocking collectives, layer(): lax.all_to_all(table.reshape(groups, -1, cols), 'sp', split_axis=0, conca...  33 us
    pallas_call x1, Pallas kernels, attention_call(): pl.pallas_call(functools.partial(attention_kernel, block=rows, score_scal...  31.6 us
    all_to_all x1, blocking collectives, layer(): lax.all_to_all(routed_out.reshape(groups, -1, cols), 'sp', split_axis=0,...  30.2 us
    all_gather x2, blocking collectives, layer(): lax.all_gather(piece, 'tp', axis=0, tiled=False)  28.2 us
    reduce_scatter x1, waiting for transfers between devices, layer(): gated = lax.psum_scatter(partial, 'tp', scatter_dimension=0, tiled=False)  26.5 us
    all_to_all x1, blocking collectives, sum_at_owner(): lax.all_to_all(cut_along(array, dim, count), axis, 0, 0, tiled=True)  24.1 us
    all_gather x1, waiting for transfers between devices, layer(): lax.all_gather(jnp.concatenate([latent_normed, packed_rot], axis=0), 'sp'...  21.2 us
  transfers between devices with their start and end apart: 11, of which 6 were waited for; matrix products, arithmetic and copies ran while one was open for 7% of the time, Pallas kernels for 3%

profile of v2, /device:TPU:0, one launch (start us, length us, event | category | flops | bytes accessed | tf_op | source)
XLA Modules:
  0.0 405.2 jit_solution(10108290241117828008)
XLA Ops:
  13.9 2.7 collective-permute-start.1
  30.1 6.7 %collective-permute-done.3 = bf16[192,576]{0,1:T(8,128)(2,1)} collective-permute-done((bf16[192,576]{0,1:T(8,128)(2,1)}, bf16[192,576]{0,1:T(8,128)(2,1)}, u32[]{:S(2)}, u32[]{:S(2)}) %collective-permute-start.3) | collective-permute-done | bytes 221216 | tf_op jit(solution)/shard_map/ppermute | solution.py:403
  38.9 6.1 %fusion.17.qt_ref = bf16[11,256,384]{2,1,0:T(8,128)(2,1)} fusion(bf16[3,64,192]{2,1,0:T(8,128)(2,1)S(1)} %get-tuple-element.42, bf16[3,64,192]{2,1,0:T(8,128)(2,1)S(1)} %get-tuple-element.41, bf16[8,64,192]{2,1,0:T(8,128)(2,1)S(1)} %copy-done.9, bf16[8,64,192]{2,1,0:T(8,128)(2,1)S(1)} %get-tuple-element.27, bf16[3,32,192]{2,1,0:T(8,128)(2,1)S(1)} %get-tuple-element.44, ...), kind=kLoop, calls=%fused_computation.24 | loop fusion | flops 42172416 | bytes 2984960 | tf_op jit(solution)/shard_map/concatenate | solution.py:433
  45.0 21.2 %all-gather.8.cloned.1.call-done = bf16[6656,512]{1,0:T(8,128)(2,1)} async-done(((bf16[208,512]{1,0:T(8,128)(2,1)}), bf16[6656,512]{1,0:T(8,128)(2,1)}) %all-gather.8.cloned.1.call-update) | async-done | bytes 6815760 | tf_op jit(solution)/shard_map/all_gather | solution.py:408
  69.4 31.6 %shard_map.199.attended_ref = bf16[11,128,192]{2,1,0:T(8,128)(2,1)S(1)} custom-call(s32[4]{0:T(128)S(1)} %pad_add_fusion.desc_ref, bf16[32,208,512]{2,1,0:T(8,128)(2,1)} %bitcast.124, bf16[11,256,384]{2,1,0:T(8,128)(2,1)S(1)} %copy-done.2, bf16[512,1024]{1,0:T(8,128)(2,1)S(1)} %copy-done.3, bf16[512,1024]{1,0:T(8,128)(2,1)S(1)} %copy-done.4), custom_call_target="tpu_custom_call" | custom-call | flops 49999998976 | bytes 12000000 | tf_op jit(solution)/shard_map/pallas_call | solution.py:318
  100.9 10.7 %collective-permute-start.4 = (bf16[3,128,192]{2,1,0:T(8,128)(2,1)S(1)}, bf16[3,128,192]{2,1,0:T(8,128)(2,1)S(1)}, u32[]{:S(2)}, u32[]{:S(2)}) collective-permute-start(bf16[3,128,192]{2,1,0:T(8,128)(2,1)S(1)} %slice.142), channel_id=1, source_target_pairs={{0,124},{4,120},{8,116},{12,112},{16,108},{20,104},{24,100},{28,96... | collective-permute-start | bytes 442376 | tf_op jit(solution)/shard_map/ppermute | solution.py:446
  111.7 4.3 %collective-permute-done.4.returned_ref = bf16[3,128,192]{2,1,0:T(8,128)(2,1)S(1)} collective-permute-done((bf16[3,128,192]{2,1,0:T(8,128)(2,1)S(1)}, bf16[3,128,192]{2,1,0:T(8,128)(2,1)S(1)}, u32[]{:S(2)}, u32[]{:S(2)}) %collective-permute-start.4) | collective-permute-done | bytes 147488 | tf_op jit(solution)/shard_map/ppermute | solution.py:446
  116.0 4.1 %shard_map.200 = bf16[192,4096]{1,0:T(8,128)(2,1)S(1)} custom-call(s32[1]{0:T(128)} %bitcast.1.own_ref, bf16[11,128,192]{2,1,0:T(8,128)(2,1)S(1)} %shard_map.199.attended_ref, bf16[3,128,192]{2,1,0:T(8,128)(2,1)S(1)} %collective-permute-done.4.returned_ref, bf16[1024,4096]{1,0:T(8,128)(2,1)S(1)} %bitcast.98), custom_call_target="tpu_custom_call" | custom-call | flops 1610612736 | bytes 11000000 | tf_op jit(solution)/shard_map/pallas_call | solution.py:78
  120.1 24.1 %all_to_all.30 = bf16[4,48,4096]{2,1,0:T(8,128)(2,1)S(1)} all-to-all(bf16[4,48,4096]{2,1,0:T(8,128)(2,1)S(1)} %bitcast.100), channel_id=1, replica_groups=mesh['sp'=32,'tp'=4] {'tp'}, dimensions={0} | all-to-all | bytes 3145728 | tf_op jit(solution)/shard_map/all_to_all | solution.py:28
  146.5 3.5 all-to-all-start.1
  150.0 5.9 %shard_map.201 = bf16[4,1536,512]{2,1,0:T(8,128)(2,1)} custom-call(bf16[1,4096,256]{2,1,0:T(8,128)(2,1)} %gate_ref.1, bf16[1,4096,256]{2,1,0:T(8,128)(2,1)} %up_ref.1, bf16[1,256,4096]{2,1,0:T(8,128)(2,1)} %down_ref.1), custom_call_target="tpu_custom_call" | custom-call | bytes 13000000 | tf_op jit(solution)/shard_map/pallas_call | solution.py:111
  157.3 5.4 %all-to-all-start.3 = ((bf16[4,1536,512]{2,1,0:T(8,128)(2,1)}), bf16[4,1536,512]{2,1,0:T(8,128)(2,1)}, u32[]{:S(2)}, u32[]{:S(2)}) async-start(bf16[4,1536,512]{2,1,0:T(8,128)(2,1)} %shard_map.201), calls=%async_computation.3 | async-start | bytes 12582912 | tf_op jit(solution)/shard_map/all_to_all | solution.py:423
  165.5 78.5 %all-to-all-done.3.w_ref = bf16[4,1536,512]{2,1,0:T(8,128)(2,1)} async-done(((bf16[4,1536,512]{2,1,0:T(8,128)(2,1)}), bf16[4,1536,512]{2,1,0:T(8,128)(2,1)}, u32[]{:S(2)}, u32[]{:S(2)}) %all-to-all-start.3) | async-done | bytes 6291488 | tf_op jit(solution)/shard_map/all_to_all | solution.py:423
  244.0 33.0 %all_to_all.31 = bf16[32,24,1024]{2,1,0:T(8,128)(2,1)} all-to-all(bf16[32,24,1024]{2,1,0:T(8,128)(2,1)} %bitcast.106), channel_id=1, replica_groups=mesh['sp'=32,'tp'=4] {'sp'}, dimensions={0} | all-to-all | bytes 3145728 | tf_op jit(solution)/shard_map/all_to_all | solution.py:462
  276.9 7.2 %shard_map.202 = bf16[4,768,512]{2,1,0:T(8,128)(2,1)} custom-call(bf16[768,1024]{1,0:T(8,128)(2,1)} %bitcast.109, bf16[4,1536,512]{2,1,0:T(8,128)(2,1)} %all-to-all-done.3.w_ref), custom_call_target="tpu_custom_call" | custom-call | flops 3221225472 | bytes 9000000 | tf_op jit(solution)/shard_map/pallas_call | solution.py:135
  284.2 2.6 fusion.46
  286.9 5.1 %convolution_convert_fusion = bf16[192,4096]{1,0:T(8,128)(2,1)} fusion(bf16[256,4096]{1,0:T(8,128)(2,1)S(1)} %copy-done, bf16[192,4096]{1,0:T(8,128)(2,1)} %all-gather.6.cloned.1.call-done, bf16[4096,256]{1,0:T(8,128)(2,1)} %param.38, f32[192,256]{1,0:T(8,128)S(1)} %fusion.46), kind=kOutput, calls=%fused_computation.6 | convolution fusion | flops 806387712 | bytes 7536640 | tf_op jit(solution)/shard_map/dot_general | solution.py:475
  292.0 26.5 %reduce-scatter.3.cloned.1.call-done = bf16[1,768,512]{2,1,0:T(8,128)(2,1)} async-done(((bf16[4,768,512]{2,1,0:T(8,128)(2,1)}), bf16[1,768,512]{2,1,0:T(8,128)(2,1)}) %reduce-scatter.3.cloned.1.call-update) | async-done | bytes 786448 | tf_op jit(solution)/shard_map/reduce_scatter | solution.py:467
  320.1 14.1 %all-gather.1 = bf16[1536,256]{1,0:T(8,128)(2,1)S(1)} all-gather(bf16[384,256]{1,0:T(8,128)(2,1)S(1)} %get-tuple-element.34), channel_id=3, replica_groups=mesh['sp'=32,'tp'=4] {'tp'}, dimensions={0}, use_global_device_ids=true | all-gather | bytes 983040 | tf_op jit(solution)/shard_map/all_gather | solution.py:479
  334.2 14.1 %all-gather.2 = bf16[1536,256]{1,0:T(8,128)(2,1)S(1)} all-gather(bf16[384,256]{1,0:T(8,128)(2,1)S(1)} %get-tuple-element.33), channel_id=4, replica_groups=mesh['sp'=32,'tp'=4] {'tp'}, dimensions={0}, use_global_device_ids=true | all-gather | bytes 983040 | tf_op jit(solution)/shard_map/all_gather | solution.py:479
  348.3 3.3 shard_map.203
  352.8 30.2 %all_to_all.32 = bf16[32,24,1024]{2,1,0:T(8,128)(2,1)S(1)} all-to-all(bf16[32,24,1024]{2,1,0:T(8,128)(2,1)} %bitcast.99), channel_id=1, replica_groups=mesh['sp'=32,'tp'=4] {'sp'}, dimensions={0} | all-to-all | bytes 3145728 | tf_op jit(solution)/shard_map/all_to_all | solution.py:485
  384.4 11.0 %all_to_all.33 = bf16[4,48,1024]{2,1,0:T(8,128)(2,1)S(1)} all-to-all(bf16[4,48,1024]{2,1,0:T(8,128)(2,1)S(1)} %bitcast.110), channel_id=1, replica_groups=mesh['sp'=32,'tp'=4] {'tp'}, dimensions={0} | all-to-all | bytes 786432 | tf_op jit(solution)/shard_map/all_to_all | solution.py:491
  396.7 2.0 fusion.27
  (138 shorter events, 36.6 us)
Async XLA Ops:
  6.5 280.3 %copy-start = (bf16[256,4096]{1,0:T(8,128)(2,1)S(1)}, bf16[256,4096]{1,0:T(8,128)(2,1)}, u32[]{:S(2)}) copy-start(bf16[256,4096]{1,0:T(8,128)(2,1)} %param.39) | copy-start | bytes 6291460
  6.5 59.7 %all-gather.8.cloned.1.call-start = ((), (), s32[]{:S(2)}) async-start(), calls=%async_computation.11 | async-start | bytes 7028736 | tf_op jit(solution)/shard_map/all_gather | solution.py:408
  7.9 11.4 %copy-start.11 = (bf16[192,1024]{1,0:T(8,128)(2,1)S(1)}, bf16[192,1024]{1,0:T(8,128)(2,1)}, u32[]{:S(2)}) copy-start(bf16[192,1024]{1,0:T(8,128)(2,1)} %param.21) | copy-start | bytes 1179652
  12.3 13.7 %collective-permute-start = (f32[48,4]{0,1:T(4,128)S(1)}, f32[48,4]{0,1:T(4,128)}, u32[]{:S(2)}, u32[]{:S(2)}) collective-permute-start(f32[48,4]{0,1:T(4,128)S(1)} %pad_maximum_fusion.5), channel_id=1, source_target_pairs={{0,1},{1,2},{2,3},{3,0},{4,5},{5,6},{6,7},{7,4},{8,9},{9,10},{10,1... | collective-permute-start | bytes 2312 | tf_op jit(solution)/shard_map/ppermute | solution.py:415
  13.9 12.1 %collective-permute-start.1 = (f32[48,4]{0,1:T(4,128)S(1)}, f32[48,4]{0,1:T(4,128)}, u32[]{:S(2)}, u32[]{:S(2)}) collective-permute-start(f32[48,4]{0,1:T(4,128)S(1)} %pad_maximum_fusion.5), channel_id=1, source_target_pairs={{0,2},{1,3},{2,0},{3,1},{4,6},{5,7},{6,4},{7,5},{8,10},{9,11},{10,... | collective-permute-start | bytes 2312 | tf_op jit(solution)/shard_map/ppermute | solution.py:415
  16.6 9.4 %collective-permute-start.2 = (f32[48,4]{0,1:T(4,128)S(1)}, f32[48,4]{0,1:T(4,128)}, u32[]{:S(2)}, u32[]{:S(2)}) collective-permute-start(f32[48,4]{0,1:T(4,128)S(1)} %pad_maximum_fusion.5), channel_id=1, source_target_pairs={{0,3},{1,0},{2,1},{3,2},{4,7},{5,4},{6,5},{7,6},{8,11},{9,8},{10,9... | collective-permute-start | bytes 2312 | tf_op jit(solution)/shard_map/ppermute | solution.py:415
  19.1 2.6 copy-start.17
  20.3 16.5 %collective-permute-start.3 = (bf16[192,576]{0,1:T(8,128)(2,1)}, bf16[192,576]{0,1:T(8,128)(2,1)}, u32[]{:S(2)}, u32[]{:S(2)}) collective-permute-start(bf16[192,576]{0,1:T(8,128)(2,1)} %pad_maximum_fusion.2), channel_id=1, source_target_pairs={{124,0},{120,4},{116,8},{112,12},{108,16},{104,20},{100,24},{96,28... | collective-permute-start | bytes 663560 | tf_op jit(solution)/shard_map/ppermute | solution.py:403
  28.1 10.7 %copy-start.9 = (bf16[8,64,192]{2,1,0:T(8,128)(2,1)S(1)}, bf16[8,64,192]{2,1,0:T(8,128)(2,1)}, u32[]{:S(2)}) copy-start(bf16[8,64,192]{2,1,0:T(8,128)(2,1)} %get-tuple-element.28) | copy-start | bytes 589828
  28.1 10.7 %copy-start.10 = (bf16[8,32,192]{2,1,0:T(8,128)(2,1)S(1)}, bf16[8,32,192]{2,1,0:T(8,128)(2,1)}, u32[]{:S(2)}) copy-start(bf16[8,32,192]{2,1,0:T(8,128)(2,1)} %get-tuple-element.40) | copy-start | bytes 294916
  28.1 10.7 %copy-start.13 = (bf16[11,256]{1,0:T(8,128)(2,1)S(1)}, bf16[11,256]{1,0:T(8,128)(2,1)}, u32[]{:S(2)}) copy-start(bf16[11,256]{1,0:T(8,128)(2,1)} %pad.26.clone) | copy-start | bytes 16900
  37.8 28.5 %copy-start.3 = (bf16[512,1024]{1,0:T(8,128)(2,1)S(1)}, bf16[512,1024]{1,0:T(8,128)(2,1)}, u32[]{:S(2)}) copy-start(bf16[512,1024]{1,0:T(8,128)(2,1)} %ku_ref.1) | copy-start | bytes 3145732
  66.2 49.7 %slice-start = ((s8[8388608]{0:T(1024)(128)(4,1)}), s8[4194304]{0:T(1024)(128)(4,1)S(1)}, s32[]{:S(2)}) async-start(s8[8388608]{0:T(1024)(128)(4,1)} %bitcast.97), calls=%async_computation.12 | async-start | bytes 8388608
  69.4 46.6 %slice-start.1 = ((s8[8388608]{0:T(1024)(128)(4,1)}), s8[4194304]{0:T(1024)(128)(4,1)S(1)}, s32[]{:S(2)}) async-start(s8[8388608]{0:T(1024)(128)(4,1)} %bitcast.97), calls=%async_computation.13 | async-start | bytes 8388608
  100.9 15.0 %collective-permute-start.4 = (bf16[3,128,192]{2,1,0:T(8,128)(2,1)S(1)}, bf16[3,128,192]{2,1,0:T(8,128)(2,1)S(1)}, u32[]{:S(2)}, u32[]{:S(2)}) collective-permute-start(bf16[3,128,192]{2,1,0:T(8,128)(2,1)S(1)} %slice.142), channel_id=1, source_target_pairs={{0,124},{4,120},{8,116},{12,112},{16,108},{20,104},{24,100},{28,96... | collective-permute-start | bytes 442376 | tf_op jit(solution)/shard_map/ppermute | solution.py:446
  145.6 10.2 %copy-start.5 = (bf16[48,4096]{1,0:T(8,128)(2,1)}, bf16[48,4096]{1,0:T(8,128)(2,1)S(1)}, u32[]{:S(2)}) copy-start(bf16[48,4096]{1,0:T(8,128)(2,1)S(1)} %fusion.26) | copy-start | bytes 1179652
  146.5 10.8 %all-to-all-start.1 = ((bf16[4,48,1024]{2,1,0:T(8,128)(2,1)}), bf16[4,48,1024]{2,1,0:T(8,128)(2,1)S(1)}, u32[]{:S(2)}, u32[]{:S(2)}) async-start(bf16[4,48,1024]{2,1,0:T(8,128)(2,1)} %pad_maximum_fusion), calls=%async_computation.1 | async-start | bytes 786432 | tf_op jit(solution)/shard_map/all_to_all | solution.py:452
  157.3 6.4 %copy-start.6 = (bf16[768,192]{0,1:T(8,128)(2,1)S(1)}, bf16[768,192]{0,1:T(8,128)(2,1)}, u32[]{:S(2)}) copy-start(bf16[768,192]{0,1:T(8,128)(2,1)} %convert_element_type.105) | copy-start | bytes 884740
  157.3 86.6 %all-to-all-start.3 = ((bf16[4,1536,512]{2,1,0:T(8,128)(2,1)}), bf16[4,1536,512]{2,1,0:T(8,128)(2,1)}, u32[]{:S(2)}, u32[]{:S(2)}) async-start(bf16[4,1536,512]{2,1,0:T(8,128)(2,1)} %shard_map.201), calls=%async_computation.3 | async-start | bytes 12582912 | tf_op jit(solution)/shard_map/all_to_all | solution.py:423
  162.7 121.4 %all-gather.6.cloned.1.call-start = ((), (), s32[]{:S(2)}) async-start(), calls=%async_computation.8 | async-start | bytes 1966080 | tf_op jit(solution)/shard_map/all_gather | solution.py:459
  163.5 155.0 %reduce-scatter.3.cloned.1.call-start = ((), (), s32[]{:S(2)}) async-start(), calls=%async_computation.9 | async-start | bytes 3932160 | tf_op jit(solution)/shard_map/reduce_scatter | solution.py:467
  284.1 111.3 %reduce-scatter.5.cloned.1.call-start = ((), (), s32[]{:S(2)}) async-start(), calls=%async_computation.10 | async-start | bytes 1966080 | tf_op jit(solution)/shard_map/reduce_scatter | solution.py:484
  352.8 30.2 %copy-start.8 = (bf16[192,768]{1,0:T(8,128)(2,1)S(1)}, bf16[192,768]{1,0:T(8,128)(2,1)}, u32[]{:S(2)}) copy-start(bf16[192,768]{1,0:T(8,128)(2,1)} %get-tuple-element.14) | copy-start | bytes 884740
  383.9 12.8 %copy-start.15 = (f32[4096]{0:T(1024)S(1)}, f32[4096]{0:T(1024)}, u32[]{:S(2)}) copy-start(f32[4096]{0:T(1024)} %param.40) | copy-start | bytes 49156
  (7 other events, 8.6 us)
Sparse Core Ops, SparseCore 0:
  11.0 55.1 all-gather.7
  165.2 42.1 all-gather.5
  284.3 34.1 reduce-scatter.2
  352.9 25.3 reduce-scatter.4
